TPU v7x, 256 devices: a whole 4x4x8 slice. The times are simulated.
256 devices in a mesh: tp: 32 (over z, y), dp: 8 (over x, core).
Axes of the slice: x: 4, y: 4, z: 8, core: 2. Of those that a mesh axis runs over, the one named last changes fastest.
Arguments:
- tokens: bfloat16 [128, 16, 4096], P('tp', None, 'dp'), may hold values from -24 to 24
- lengths: int32 [128], P('dp'), may hold values from 1 to 16, 896 in all
- norm_gain: float32 [2, 4096], P(None, 'dp'), may hold values from 0.1 to 1.9
- query_weight: bfloat16 [2, 4096, 4096], P(None, 'dp', 'tp'), may hold values from -0.09375 to 0.09375
- key_weight: bfloat16 [2, 4096, 4096], P(None, 'dp', 'tp'), may hold values from -0.09375 to 0.09375
- value_weight: bfloat16 [2, 4096, 4096], P(None, 'dp', 'tp'), may hold values from -0.09375 to 0.09375
- outgate_weight: bfloat16 [2, 4096, 4096], P(None, 'dp', 'tp'), may hold values from -0.09375 to 0.09375
- input_gate_weight: bfloat16 [2, 4096, 32], replicated, may hold values from -0.09375 to 0.09375
- forget_gate_weight: bfloat16 [2, 4096, 32], replicated, may hold values from -0.09375 to 0.09375
- forget_bias: float32 [2, 32], P(None, 'tp'), may hold values from -1 to 6
- out_weight: bfloat16 [2, 4096, 4096], P(None, 'tp', 'dp'), may hold values from -0.09375 to 0.09375
- cell_state: float32 [2, 128, 32, 128, 128], P(None, 'dp', 'tp'), may hold values from -1.5 to 1.5
- norm_state: float32 [2, 128, 32, 128], P(None, 'dp', 'tp'), may hold values from -1.5 to 1.5
- max_state: float32 [2, 128, 32], P(None, 'dp', 'tp'), may hold values from -6 to 6
Outputs:
- tokens_next: bfloat16 [128, 16, 4096], P('tp', None, 'dp')
- cell_next: float32 [2, 128, 32, 128, 128], P(None, 'dp', 'tp')
- norm_next: float32 [2, 128, 32, 128], P(None, 'dp', 'tp')
- max_next: float32 [2, 128, 32], P(None, 'dp', 'tp')
Inputs may be any that keep to these rules, and one draw needn't show every extreme that they name: `lengths`: the largest is 16.
All inputs are finite; a program needn't handle non-finite values. No bound on the sum of `lengths` on one device may be relied on, other than what follows from the above.
Results may differ from a plain program's by a relative error of at most 0.025.
Values may be sent and summed in bfloat16 or wider, within the bound.
No kernel may reach another device: no remote copies, remote signals or barrier semaphores. Data moves between devices by JAX's collectives and lax.ppermute only.
A program may use at most 64 MiB of HBM per device.

v0:
```python
import jax
import jax.numpy as jnp
from jax import lax
from jax.sharding import Mesh
from jax.sharding import PartitionSpec as P

TP = ("tp_0", "tp_1")


EPSILON = 1e-06
NEG_FILL = -1e30


def whole_of(array, axes, dim):
    whole = array
    for number in range(len(axes) - 1, -1, -1):
        whole = lax.all_gather(whole, axes[number], axis=dim, tiled=True)
    return whole


def in_one_piece(arrays, axis, dim, along):
    both = jnp.concatenate(arrays, axis=along)
    whole, at, finished = (lax.psum_scatter(both, axis, scatter_dimension=dim, tiled=True), 0, [])
    for a in arrays:
        finished.append(lax.slice_in_dim(whole, at, at + a.shape[along], axis=along))
        at += a.shape[along]
    return tuple(finished)


def in_blocks(array, dim, size):
    before, after = (array.shape[:dim], array.shape[dim + 1 :])
    return jnp.moveaxis(array.reshape(*before, size, -1, *after), dim, 0)


def summed_on_arrival(array, axis, dim):
    parts = in_blocks(array, dim, lax.axis_size(axis))
    arrived = lax.all_to_all(parts, axis, split_axis=0, concat_axis=0, tiled=True)
    return arrived.sum(axis=0)


def in_order(parts, dim):
    dims = list(parts.shape[1:])
    dims[dim] *= parts.shape[0]
    return jnp.moveaxis(parts, 0, dim).reshape(dims)


def from_everyone(array, axis):
    size = lax.axis_size(axis)
    return lax.all_to_all(
        jnp.broadcast_to(array[None], (size, *array.shape)), axis, 0, 0, tiled=True
    )


def gathered_copies(array, axis, dim):
    return in_order(from_everyone(array, axis), dim)


def cell_update(cell, normer, stabil, query, key_vec, value, in_gate, log_forget, live):
    high = lax.Precision.HIGHEST
    in_gate = jnp.where(live, in_gate, NEG_FILL)
    log_forget = jnp.where(live, log_forget, 0.0)
    cumul = jnp.cumsum(log_forget, axis=-1)
    span = query.shape[2]
    causal = jnp.tril(jnp.ones((span, span), dtype=bool))
    log_weight = jnp.where(
        causal, cumul[..., :, None] - cumul[..., None, :] + in_gate[..., None, :], NEG_FILL
    )
    carried = cumul + stabil[..., None]
    running = jnp.maximum(jnp.max(log_weight, axis=-1), carried)
    carry_scale = jnp.exp(carried - running)
    scores = jnp.einsum("bhtd,bhud->bhtu", query, key_vec, precision=high) * jnp.exp(
        log_weight - running[..., None]
    )
    numer = jnp.einsum("bhtu,bhue->bhte", scores, value, precision=high)
    numer = numer + carry_scale[..., None] * jnp.einsum(
        "bhtd,bhde->bhte", query, cell, precision=high
    )
    denom = jnp.sum(scores, axis=-1) + carry_scale * jnp.einsum(
        "bhtd,bhd->bht", query, normer, precision=high
    )
    readout = numer / jnp.maximum(jnp.abs(denom), 1.0)[..., None]
    readout = jnp.where(live[..., None], readout, 0.0)
    stabil_next = running[..., -1]
    source_weight = jnp.exp(cumul[..., -1:] - cumul + in_gate - stabil_next[..., None])
    decay = jnp.exp(cumul[..., -1] + stabil - stabil_next)
    cell_next = decay[..., None, None] * cell + jnp.einsum(
        "bhu,bhud,bhue->bhde", source_weight, key_vec, value, precision=high
    )
    normer_next = decay[..., None] * normer + jnp.einsum(
        "bhu,bhud->bhd", source_weight, key_vec, precision=high
    )
    return (cell_next, normer_next, stabil_next, readout)


def to_heads(flat, seqs, span, heads):
    return jnp.transpose(flat.reshape(seqs, span, heads, -1), (0, 2, 1, 3)).astype(jnp.float32)


def per_device(
    tokens,
    lengths,
    norm_gain,
    query_weight,
    key_weight,
    value_weight,
    outgate_weight,
    input_gate_weight,
    forget_gate_weight,
    forget_bias,
    out_weight,
    cell_state,
    norm_state,
    max_state,
):
    seq_here, span, feat_here = tokens.shape
    local_seqs = cell_state.shape[1]
    heads_here = cell_state.shape[2]
    head_size = cell_state.shape[3]
    width = feat_here * lax.axis_size("dp")
    row_start = lax.axis_index("dp") * feat_here
    head_start = lax.axis_index(TP) * heads_here
    live = (jnp.arange(span, dtype=jnp.int32)[None, :] < lengths[:, None])[:, None, :]
    current = tokens
    cells, normers, stabils = ([], [], [])
    for layer_index in range(2):
        gathered = whole_of(current, TP, 0)
        all_seqs = gathered.shape[0]
        widened = gathered.reshape(all_seqs * span, feat_here).astype(jnp.float32)
        squares = jnp.sum(widened * widened, axis=-1)
        scaled = (widened * norm_gain[layer_index]).astype(jnp.bfloat16)
        gate_columns = jnp.concatenate(
            [
                lax.dynamic_slice(
                    input_gate_weight[layer_index], (row_start, head_start), (feat_here, heads_here)
                ),
                lax.dynamic_slice(
                    forget_gate_weight[layer_index],
                    (row_start, head_start),
                    (feat_here, heads_here),
                ),
            ],
            axis=1,
        )

        def partial_sum(weight):
            part = jnp.dot(scaled, weight, preferred_element_type=jnp.float32)
            return lax.optimization_barrier(part.astype(jnp.bfloat16)).astype(jnp.float32)

        sums = tuple(
            (
                part.astype(jnp.float32)
                for part in in_one_piece(
                    (
                        partial_sum(query_weight[layer_index]).astype(jnp.bfloat16),
                        partial_sum(key_weight[layer_index]).astype(jnp.bfloat16),
                        partial_sum(value_weight[layer_index]).astype(jnp.bfloat16),
                        partial_sum(outgate_weight[layer_index]).astype(jnp.bfloat16),
                        partial_sum(gate_columns).astype(jnp.bfloat16),
                    ),
                    "dp",
                    0,
                    1,
                )
            )
        )
        totals = summed_on_arrival(squares, "dp", 0)
        scale = lax.rsqrt(totals[:, None] / width + EPSILON)
        query = to_heads((scale * sums[0]).astype(jnp.bfloat16), local_seqs, span, heads_here)
        key_vec = to_heads(
            (scale * sums[1]).astype(jnp.bfloat16), local_seqs, span, heads_here
        ) * head_size ** (-0.5)
        value = to_heads((scale * sums[2]).astype(jnp.bfloat16), local_seqs, span, heads_here)
        outgate = (scale * sums[3]).astype(jnp.bfloat16).astype(jnp.float32)
        gate_both = scale * sums[4]
        in_gate = jnp.transpose(
            gate_both[:, :heads_here].reshape(local_seqs, span, heads_here), (0, 2, 1)
        )
        log_forget = jax.nn.log_sigmoid(
            jnp.transpose(
                gate_both[:, heads_here:].reshape(local_seqs, span, heads_here)
                + forget_bias[layer_index],
                (0, 2, 1),
            )
        )
        cell_next, normer_next, stabil_next, readout = cell_update(
            cell_state[layer_index],
            norm_state[layer_index],
            max_state[layer_index],
            query,
            key_vec,
            value,
            in_gate,
            log_forget,
            live,
        )
        cells.append(cell_next)
        normers.append(normer_next)
        stabils.append(stabil_next)
        readout = jnp.transpose(readout, (0, 2, 1, 3)).reshape(
            local_seqs * span, heads_here * head_size
        )
        gated = (
            (readout * jax.nn.sigmoid(outgate))
            .astype(jnp.bfloat16)
            .reshape(local_seqs, span, heads_here * head_size)
        )
        everyone = gathered_copies(gated, "dp", 0)
        weight_here = out_weight[layer_index]
        regrouped = lax.all_to_all(everyone, TP, split_axis=0, concat_axis=2, tiled=True)
        rows_flat = regrouped.reshape(seq_here * span, regrouped.shape[2])
        mixed = jnp.dot(rows_flat, whole_of(weight_here, TP, 0), preferred_element_type=jnp.float32)
        own = current.reshape(seq_here * span, feat_here).astype(jnp.float32)
        current = (own + mixed).astype(jnp.bfloat16).reshape(seq_here, span, feat_here)
    return (current, jnp.stack(cells), jnp.stack(normers), jnp.stack(stabils))


def solution(mesh):
    finer = Mesh(mesh.devices.reshape(8, 4, mesh.shape["dp"]), ("tp_0", "tp_1", "dp"))
    placed = (
        P(TP, None, "dp"),
        P("dp"),
        P(None, "dp"),
        P(None, "dp", TP),
        P(None, "dp", TP),
        P(None, "dp", TP),
        P(None, "dp", TP),
        P(),
        P(),
        P(None, TP),
        P(None, TP, "dp"),
        P(None, "dp", TP, None, None),
        P(None, "dp", TP, None),
        P(None, "dp", TP),
    )
    return jax.shard_map(
        per_device,
        mesh=finer,
        in_specs=placed,
        out_specs=(
            P(TP, None, "dp"),
            P(None, "dp", TP, None, None),
            P(None, "dp", TP, None),
            P(None, "dp", TP),
        ),
        check_vma=False,
    )
```

profile of v0, /device:TPU:1, one launch (start us, length us, event | category | flops | bytes accessed | tf_op | source)
XLA Modules:
  0.0 362.8 jit_solution(9765050597729144626)
XLA Ops:
  7.2 12.7 %all_gather.24 = bf16[16,16,512]{2,1,0:T(8,128)(2,1)} all-gather(bf16[4,16,512]{2,1,0:T(8,128)(2,1)} %param.14), channel_id=1, replica_groups=mesh['tp_0'=8,'tp_1'=4,'dp'=8] {'tp_1'}, dimensions={0}, use_global_device_ids=true | all-gather | bytes 327680 | tf_op jit(solution)/shard_map/all_gather | solution.py:17
  20.0 1.8 fusion.80
  21.8 1.8 fusion.81
  24.2 36.7 %all-gather.9.cloned.1.call-done = bf16[128,16,512]{2,1,0:T(8,128)(2,1)} async-done(((bf16[16,16,512]{2,1,0:T(8,128)(2,1)}), bf16[128,16,512]{2,1,0:T(8,128)(2,1)}) %all-gather.9.cloned.1.call-update) | async-done | bytes 2097168 | tf_op jit(solution)/shard_map/all_gather | solution.py:17
  60.9 2.0 fusion.5
  69.1 1.4 copy-done.3
  70.7 11.6 %all-gather = bf16[1,512,512]{2,1,0:T(8,128)(2,1)} all-gather(bf16[1,128,512]{2,1,0:T(8,128)(2,1)S(1)} %get-tuple-element.60), channel_id=2, replica_groups=mesh['tp_0'=8,'tp_1'=4,'dp'=8] {'tp_1'}, dimensions={1}, use_global_device_ids=true | all-gather | bytes 655360 | tf_op jit(solution)/shard_map/all_gather | solution.py:17
  84.8 12.0 %all-to-all-start = ((f32[8,1,256]{2,1,0:T(1,128)}), f32[8,1,256]{2,1,0:T(1,128)S(1)}, u32[]{:S(2)}, u32[]{:S(2)}) async-start(f32[8,1,256]{2,1,0:T(1,128)} %all_to_all.52), calls=%async_computation | async-start | bytes 16384 | tf_op jit(solution)/shard_map/all_to_all | solution.py:37
  97.0 4.4 %all-to-all-done = f32[8,1,256]{2,1,0:T(1,128)S(1)} async-done(((f32[8,1,256]{2,1,0:T(1,128)}), f32[8,1,256]{2,1,0:T(1,128)S(1)}, u32[]{:S(2)}, u32[]{:S(2)}) %all-to-all-start) | async-done | bytes 8224 | tf_op jit(solution)/shard_map/all_to_all | solution.py:37
  101.4 7.0 %reduce-scatter.3.cloned.1.call-done = bf16[256,514]{1,0:T(8,128)(2,1)} async-done(((bf16[2048,514]{1,0:T(8,128)(2,1)}), bf16[256,514]{1,0:T(8,128)(2,1)}) %reduce-scatter.3.cloned.1.call-update) | async-done | bytes 263184 | tf_op jit(solution)/shard_map/reduce_scatter | solution.py:23
  115.9 15.2 %all_to_all.60 = bf16[8,16,16,128]{3,2,1,0:T(8,128)(2,1)S(1)} all-to-all(bf16[8,16,16,128]{3,2,1,0:T(8,128)(2,1)S(1)} %broadcast_in_dim.87), channel_id=1, replica_groups=mesh['tp_0'=8,'tp_1'=4,'dp'=8] {'dp'}, dimensions={0} | all-to-all | bytes 1048576 | tf_op jit(solution)/shard_map/all_to_all | solution.py:49
  131.1 31.5 %all_to_all.61 = bf16[128,16,128]{2,1,0:T(8,128)(2,1)S(1)} all-to-all(bf16[128,16,128]{2,1,0:T(8,128)(2,1)S(1)} %bitcast.225), channel_id=1, replica_groups=mesh['tp_0'=8,'tp_1'=4,'dp'=8] {'tp_0','tp_1'}, dimensions={0} | all-to-all | bytes 1048576 | tf_op jit(solution)/shard_map/all_to_all | solution.py:209
  162.9 14.6 %all-gather.13.cloned.1.call-done = bf16[1,4096,512]{2,1,0:T(8,128)(2,1)} async-done(((bf16[1,512,512]{2,1,0:T(8,128)(2,1)}), bf16[1,4096,512]{2,1,0:T(8,128)(2,1)}) %all-gather.13.cloned.1.call-update) | async-done | bytes 4194320 | tf_op jit(solution)/shard_map/all_gather | solution.py:17
  177.5 2.9 fusion.21
  180.4 10.8 %all_gather.28 = bf16[16,16,512]{2,1,0:T(8,128)(2,1)} all-gather(bf16[4,16,512]{2,1,0:T(8,128)(2,1)S(1)} %bitcast.227), channel_id=1, replica_groups=mesh['tp_0'=8,'tp_1'=4,'dp'=8] {'tp_1'}, dimensions={0}, use_global_device_ids=true | all-gather | bytes 327680 | tf_op jit(solution)/shard_map/all_gather | solution.py:17
  192.9 36.0 %all-gather.11.cloned.1.call-done = bf16[128,16,512]{2,1,0:T(8,128)(2,1)} async-done(((bf16[16,16,512]{2,1,0:T(8,128)(2,1)}), bf16[128,16,512]{2,1,0:T(8,128)(2,1)}) %all-gather.11.cloned.1.call-update) | async-done | bytes 2097168 | tf_op jit(solution)/shard_map/all_gather | solution.py:17
  228.9 2.3 multiply_reduce_fusion
  232.1 1.5 convolution_convert_fusion.2
  233.6 1.5 convolution_convert_fusion.1
  239.7 1.9 constant_dynamic-update-slice_fusion.8
  241.6 2.0 constant_dynamic-update-slice_fusion.7
  245.5 11.5 %all-gather.2 = bf16[1,512,512]{2,1,0:T(8,128)(2,1)} all-gather(bf16[1,128,512]{2,1,0:T(8,128)(2,1)S(1)} %get-tuple-element.61), channel_id=4, replica_groups=mesh['tp_0'=8,'tp_1'=4,'dp'=8] {'tp_1'}, dimensions={1}, use_global_device_ids=true | all-gather | bytes 655360 | tf_op jit(solution)/shard_map/all_gather | solution.py:17
  257.7 11.9 %all-to-all-start.3 = ((f32[8,1,256]{2,1,0:T(1,128)}), f32[8,1,256]{2,1,0:T(1,128)S(1)}, u32[]{:S(2)}, u32[]{:S(2)}) async-start(f32[8,1,256]{2,1,0:T(1,128)} %all_to_all.53), calls=%async_computation.4 | async-start | bytes 16384 | tf_op jit(solution)/shard_map/all_to_all | solution.py:37
  269.8 4.6 %all-to-all-done.3 = f32[8,1,256]{2,1,0:T(1,128)S(1)} async-done(((f32[8,1,256]{2,1,0:T(1,128)}), f32[8,1,256]{2,1,0:T(1,128)S(1)}, u32[]{:S(2)}, u32[]{:S(2)}) %all-to-all-start.3) | async-done | bytes 8224 | tf_op jit(solution)/shard_map/all_to_all | solution.py:37
  274.4 9.1 %reduce-scatter.5.cloned.1.call-done = bf16[256,514]{1,0:T(8,128)(2,1)} async-done(((bf16[2048,514]{1,0:T(8,128)(2,1)}), bf16[256,514]{1,0:T(8,128)(2,1)}) %reduce-scatter.5.cloned.1.call-update) | async-done | bytes 263184 | tf_op jit(solution)/shard_map/reduce_scatter | solution.py:23
  290.6 7.2 %all-to-all-start.4 = ((bf16[8,16,16,128]{3,2,1,0:T(8,128)(2,1)}), bf16[8,16,16,128]{3,2,1,0:T(8,128)(2,1)}, u32[]{:S(2)}, u32[]{:S(2)}) async-start(bf16[8,16,16,128]{3,2,1,0:T(8,128)(2,1)} %broadcast_in_dim.89), calls=%async_computation.6 | async-start | bytes 1048576 | tf_op jit(solution)/shard_map/all_to_all | solution.py:49
  298.9 8.4 %all-to-all-done.4 = bf16[8,16,16,128]{3,2,1,0:T(8,128)(2,1)} async-done(((bf16[8,16,16,128]{3,2,1,0:T(8,128)(2,1)}), bf16[8,16,16,128]{3,2,1,0:T(8,128)(2,1)}, u32[]{:S(2)}, u32[]{:S(2)}) %all-to-all-start.4) | async-done | bytes 524320 | tf_op jit(solution)/shard_map/all_to_all | solution.py:49
  307.3 9.5 %all-to-all-start.5 = ((bf16[128,16,128]{2,1,0:T(8,128)(2,1)}), bf16[128,16,128]{2,1,0:T(8,128)(2,1)S(1)}, u32[]{:S(2)}, u32[]{:S(2)}) async-start(bf16[128,16,128]{2,1,0:T(8,128)(2,1)} %bitcast.56), calls=%async_computation.7 | async-start | bytes 1048576 | tf_op jit(solution)/shard_map/all_to_all | solution.py:209
  319.8 1.5 maximum_bitcast_fusion
  321.3 17.9 %all-to-all-done.5 = bf16[128,16,128]{2,1,0:T(8,128)(2,1)S(1)} async-done(((bf16[128,16,128]{2,1,0:T(8,128)(2,1)}), bf16[128,16,128]{2,1,0:T(8,128)(2,1)S(1)}, u32[]{:S(2)}, u32[]{:S(2)}) %all-to-all-start.5) | async-done | bytes 524320 | tf_op jit(solution)/shard_map/all_to_all | solution.py:209
  339.5 12.9 %all-gather.15.cloned.1.call-done = bf16[1,4096,512]{2,1,0:T(8,128)(2,1)} async-done(((bf16[1,512,512]{2,1,0:T(8,128)(2,1)}), bf16[1,4096,512]{2,1,0:T(8,128)(2,1)}) %all-gather.15.cloned.1.call-update) | async-done | bytes 4194320 | tf_op jit(solution)/shard_map/all_gather | solution.py:17
  352.4 3.5 fusion.18
  (177 shorter events, 38.4 us)
Async XLA Ops:
  7.2 16.4 %copy-start.33 = (f32[2,512]{1,0:T(2,128)S(1)}, f32[2,512]{1,0:T(2,128)}, u32[]{:S(2)}) copy-start(f32[2,512]{1,0:T(2,128)} %param.16) | copy-start | bytes 12292
  7.2 53.7 %all-gather.9.cloned.1.call-start = ((), (), s32[]{:S(2)}) async-start(), calls=%async_computation.8 | async-start | bytes 2359296 | tf_op jit(solution)/shard_map/all_gather | solution.py:17
  19.9 88.5 %reduce-scatter.3.cloned.1.call-start = ((), (), s32[]{:S(2)}) async-start(), calls=%async_computation.9 | async-start | bytes 2949120 | tf_op jit(solution)/shard_map/reduce_scatter | solution.py:23
  69.1 13.3 %copy-start.39 = (f32[2,1]{0,1:T(1,128)S(1)}, f32[2,1]{0,1:T(1,128)}, u32[]{:S(2)}) copy-start(f32[2,1]{0,1:T(1,128)} %param.23) | copy-start | bytes 28
  69.1 13.8 %copy-start.34 = (f32[2,16,1]{1,2,0:T(1,128)S(1)}, f32[2,16,1]{1,2,0:T(1,128)}, u32[]{:S(2)}) copy-start(f32[2,16,1]{1,2,0:T(1,128)} %param.27) | copy-start | bytes 388
  69.1 14.3 %copy-start.16 = (s32[16]{0:T(128)S(1)}, s32[16]{0:T(128)}, u32[]{:S(2)}) copy-start(s32[16]{0:T(128)} %param.15) | copy-start | bytes 196
  69.1 14.4 %copy-start.14 = (f32[2,16,1,128]{3,2,1,0:T(1,128)S(1)}, f32[2,16,1,128]{3,2,1,0:T(1,128)}, u32[]{:S(2)}) copy-start(f32[2,16,1,128]{3,2,1,0:T(1,128)} %param.26) | copy-start | bytes 49156
  70.6 43.3 %copy-start = (f32[2,16,1,128,128]{4,3,2,1,0:T(8,128)S(1)}, f32[2,16,1,128,128]{4,3,2,1,0:T(8,128)}, u32[]{:S(2)}) copy-start(f32[2,16,1,128,128]{4,3,2,1,0:T(8,128)} %param.25) | copy-start | bytes 6291460
  70.6 106.9 %all-gather.13.cloned.1.call-start = ((), (), s32[]{:S(2)}) async-start(), calls=%async_computation.12 | async-start | bytes 4718592 | tf_op jit(solution)/shard_map/all_gather | solution.py:17
  83.5 32.4 %copy-start.37 = (pred[16,16]{1,0:T(8,128)(4,1)}, pred[16,16]{1,0:T(8,128)(4,1)S(1)}, u32[]{:S(2)}) copy-start(pred[16,16]{1,0:T(8,128)(4,1)S(1)} %iota_compare_fusion.2) | copy-start | bytes 772
  84.8 16.6 %all-to-all-start = ((f32[8,1,256]{2,1,0:T(1,128)}), f32[8,1,256]{2,1,0:T(1,128)S(1)}, u32[]{:S(2)}, u32[]{:S(2)}) async-start(f32[8,1,256]{2,1,0:T(1,128)} %all_to_all.52), calls=%async_computation | async-start | bytes 16384 | tf_op jit(solution)/shard_map/all_to_all | solution.py:37
  96.8 132.1 %all-gather.11.cloned.1.call-start = ((), (), s32[]{:S(2)}) async-start(), calls=%async_computation.10 | async-start | bytes 2359296 | tf_op jit(solution)/shard_map/all_gather | solution.py:17
  96.8 19.1 %copy-start.24 = (pred[16,16]{0,1:T(8,128)(4,1)}, pred[16,16]{0,1:T(8,128)(4,1)S(1)}, u32[]{:S(2)}) copy-start(pred[16,16]{0,1:T(8,128)(4,1)S(1)} %iota_compare_fusion.1) | copy-start | bytes 772
  96.9 14.8 %copy-start.20 = (pred[16,16]{1,0:T(8,128)(4,1)}, pred[16,16]{1,0:T(8,128)(4,1)S(1)}, u32[]{:S(2)}) copy-start(pred[16,16]{1,0:T(8,128)(4,1)S(1)} %copy.90) | copy-start | bytes 772
  114.8 62.7 %copy-start.4 = (bf16[4,16,512]{2,1,0:T(8,128)(2,1)S(1)}, bf16[4,16,512]{2,1,0:T(8,128)(2,1)}, u32[]{:S(2)}) copy-start(bf16[4,16,512]{2,1,0:T(8,128)(2,1)} %param.14) | copy-start | bytes 196612
  177.5 51.4 %copy-start.18 = (f32[1,512]{1,0:T(1,128)S(1)}, f32[1,512]{1,0:T(1,128)}, u32[]{:S(2)}) copy-start(f32[1,512]{1,0:T(1,128)} %get-tuple-element.71) | copy-start | bytes 6148
  191.3 92.2 %reduce-scatter.5.cloned.1.call-start = ((), (), s32[]{:S(2)}) async-start(), calls=%async_computation.11 | async-start | bytes 2949120 | tf_op jit(solution)/shard_map/reduce_scatter | solution.py:23
  245.4 24.3 %copy-start.40 = (f32[16,1,1]{0,2,1:T(1,128)S(1)}, f32[16,1,1]{0,2,1:T(1,128)}, u32[]{:S(2)}) copy-start(f32[16,1,1]{0,2,1:T(1,128)} %get-tuple-element.75) | copy-start | bytes 196
  245.4 39.9 %copy-start.17 = (s32[16]{0:T(128)S(1)}, s32[16]{0:T(128)}, u32[]{:S(2)}) copy-start(s32[16]{0:T(128)} %param.15) | copy-start | bytes 196
  245.4 40.3 %copy-start.21 = (pred[16,16]{1,0:T(8,128)(4,1)S(1)}, pred[16,16]{1,0:T(8,128)(4,1)}, u32[]{:S(2)}) copy-start(pred[16,16]{1,0:T(8,128)(4,1)} %copy-done.20) | copy-start | bytes 772
  245.4 40.5 %copy-start.23 = (f32[16]{0:T(128)S(1)}, f32[16]{0:T(128)}, u32[]{:S(2)}) copy-start(f32[16]{0:T(128)} %get-tuple-element.76) | copy-start | bytes 196
  245.4 41.8 %copy-start.28 = (f32[1,16,1,128]{3,1,2,0:T(8,128)S(1)}, f32[1,16,1,128]{3,1,2,0:T(8,128)}, u32[]{:S(2)}) copy-start(f32[1,16,1,128]{3,1,2,0:T(8,128)} %get-tuple-element.64) | copy-start | bytes 24580
  245.4 42.0 %copy-start.25 = (pred[16,16]{0,1:T(8,128)(4,1)S(1)}, pred[16,16]{0,1:T(8,128)(4,1)}, u32[]{:S(2)}) copy-start(pred[16,16]{0,1:T(8,128)(4,1)} %copy-done.24) | copy-start | bytes 772
  245.5 107.0 %all-gather.15.cloned.1.call-start = ((), (), s32[]{:S(2)}) async-start(), calls=%async_computation.13 | async-start | bytes 4718592 | tf_op jit(solution)/shard_map/all_gather | solution.py:17
  245.5 42.9 %copy-start.38 = (pred[16,16]{1,0:T(8,128)(4,1)S(1)}, pred[16,16]{1,0:T(8,128)(4,1)}, u32[]{:S(2)}) copy-start(pred[16,16]{1,0:T(8,128)(4,1)} %copy-done.37) | copy-start | bytes 772
  257.7 16.6 %all-to-all-start.3 = ((f32[8,1,256]{2,1,0:T(1,128)}), f32[8,1,256]{2,1,0:T(1,128)S(1)}, u32[]{:S(2)}, u32[]{:S(2)}) async-start(f32[8,1,256]{2,1,0:T(1,128)} %all_to_all.53), calls=%async_computation.4 | async-start | bytes 16384 | tf_op jit(solution)/shard_map/all_to_all | solution.py:37
  288.4 28.4 %copy-start.36 = (f32[16]{0:T(128)S(1)}, f32[16]{0:T(128)}, u32[]{:S(2)}) copy-start(f32[16]{0:T(128)} %get-tuple-element.32) | copy-start | bytes 196
  288.4 29.1 %copy-start.32 = (f32[16]{0:T(128)S(1)}, f32[16]{0:T(128)}, u32[]{:S(2)}) copy-start(f32[16]{0:T(128)} %copy-done.31) | copy-start | bytes 196
  288.4 29.1 %copy-start.35 = (f32[2,16,1]{1,2,0:T(1,128)S(1)}, f32[2,16,1]{1,2,0:T(1,128)}, u32[]{:S(2)}) copy-start(f32[2,16,1]{1,2,0:T(1,128)} %param.27) | copy-start | bytes 388
  288.4 29.1 %copy-start.15 = (f32[16,16]{1,0:T(8,128)S(1)}, f32[16,16]{1,0:T(8,128)}, u32[]{:S(2)}) copy-start(f32[16,16]{1,0:T(8,128)} %get-tuple-element.38) | copy-start | bytes 3076
  290.6 16.7 %all-to-all-start.4 = ((bf16[8,16,16,128]{3,2,1,0:T(8,128)(2,1)}), bf16[8,16,16,128]{3,2,1,0:T(8,128)(2,1)}, u32[]{:S(2)}, u32[]{:S(2)}) async-start(bf16[8,16,16,128]{3,2,1,0:T(8,128)(2,1)} %broadcast_in_dim.89), calls=%async_computation.6 | async-start | bytes 1048576 | tf_op jit(solution)/shard_map/all_to_all | solution.py:49
  307.3 31.9 %all-to-all-start.5 = ((bf16[128,16,128]{2,1,0:T(8,128)(2,1)}), bf16[128,16,128]{2,1,0:T(8,128)(2,1)S(1)}, u32[]{:S(2)}, u32[]{:S(2)}) async-start(bf16[128,16,128]{2,1,0:T(8,128)(2,1)} %bitcast.56), calls=%async_computation.7 | async-start | bytes 1048576 | tf_op jit(solution)/shard_map/all_to_all | solution.py:209
  (19 other events, 47.7 us)
Sparse Core Ops, SparseCore 0:
  20.0 40.8 all-gather.8
  70.7 37.6 reduce-scatter.2
  110.2 67.2 all-gather.12
  191.4 37.4 all-gather.10
  245.6 37.8 reduce-scatter.4
  285.1 67.2 all-gather.14
where the time goes:
time: 364 us; the launch traced here: 363 us
  waiting for transfers between devices  152 us (42%)
  blocking collectives  93.3 us (26%)
  starting transfers between devices  41 us (11%)
  local copies, waits for them, and re-layouts  22.4 us (6%)
  matrix products  21 us (6%)
  other arithmetic  18.7 us (5%)
  between operations  14.7 us (4%)
    all_gather x4, waiting for transfers between devices, whole_of(): whole = lax.all_gather(whole, axes[number], axis=dim, tiled=True)  100 us
    all_gather x4, blocking collectives, whole_of(): whole = lax.all_gather(whole, axes[number], axis=dim, tiled=True)  46.6 us
    all_to_all x1, blocking collectives, per_device(): lax.all_to_all(everyone, TP, split_axis=0, concat_axis=2, tiled=True)  31.5 us
    all_to_all x2, starting transfers between devices, summed_on_arrival(): lax.all_to_all(parts, axis, split_axis=0, concat_axis=0, tiled=True)  23.9 us
    all_to_all x1, waiting for transfers between devices, per_device(): lax.all_to_all(everyone, TP, split_axis=0, concat_axis=2, tiled=True)  17.9 us
    reduce_scatter x2, waiting for transfers between devices, in_one_piece(): lax.psum_scatter(both, axis, scatter_dimension=dim, tiled=True)  16.1 us
    all_to_all x1, blocking collectives, from_everyone(): lax.all_to_all(jnp.broadcast_to(array[None], (size, *array.shape)), axis,...  15.2 us
    all_to_all x1, starting transfers between devices, per_device(): lax.all_to_all(everyone, TP, split_axis=0, concat_axis=2, tiled=True)  9.49 us
  transfers between devices with their start and end apart: 10, of which 10 were waited for; matrix products, arithmetic and copies ran while one was open for 8% of the time, Pallas kernels for 0%

commit v1 on v0

v1 whole, which is shorter than its diff:
```python
import jax
import jax.numpy as jnp
from jax import lax
from jax.experimental import pallas as pl
from jax.experimental.pallas import tpu as pltpu
from jax.sharding import Mesh
from jax.sharding import PartitionSpec as P

TP = ("zh", "zl", "y")
DP = ("x", "c")
ZZ = ("zl", "zh")
YX = ("y", "x")

EPSILON = 1e-06
NEG_FILL = -1e30
F32 = jnp.float32
BF16 = jnp.bfloat16
EXTRA = 8


def split_pair(value):
    high = value.astype(BF16)
    return high, (value - high.astype(F32)).astype(BF16)


def dot(a, b):
    return lax.dot_general(a, b, (((1,), (0,)), ((), ())), preferred_element_type=F32)


def dot_nt(a, b):
    return lax.dot_general(a, b, (((1,), (1,)), ((), ())), preferred_element_type=F32)


def project_kernel(where, tokens, gain, gates, *rest):
    weights, out = rest[:-1], rest[-1]
    y, c = where[0], where[1]
    ny = len(weights) // 2
    nx, toks, feat = tokens.shape[1:]
    halves = []
    squares = []
    for half in (c, 1 - c):
        wide = tokens[half].reshape(nx * toks, feat).astype(F32)
        halves.append((wide * gain[pl.ds(half, 1), :]).astype(BF16))
        squares.append(split_pair(wide * wide))
    gate_half = [gates[c], gates[1 - c]]
    ones = jnp.ones((8, feat), BF16)
    extras = []
    for xi in range(nx):
        rows = slice(xi * toks, (xi + 1) * toks)
        both = dot_nt(gate_half[0], halves[0][rows]) + dot_nt(gate_half[1], halves[1][rows])
        square = sum(dot_nt(ones, part[rows]) for pair in squares for part in pair)
        extras.append((both, square))
    for k in range(ny):
        head = lax.rem(y + ny - k, ny)
        done = dot(halves[0], weights[2 * k][...]) + dot(halves[1], weights[2 * k + 1][...])
        out[head, :, :toks, :] = done.astype(BF16).reshape(nx, toks, done.shape[1])
    out[:, :, toks:, :] = jnp.zeros((ny, nx, EXTRA, out.shape[3]), BF16)
    for xi in range(nx):
        both, square = extras[xi]
        high, low = (p.astype(F32) for p in split_pair(both))
        s_high, s_low = (p.astype(F32) for p in split_pair(square))
        for head in range(ny):
            a, b = 2 * head, 2 * head + 1
            block = jnp.concatenate(
                [
                    high[a : a + 1],
                    low[a : a + 1],
                    high[b : b + 1],
                    low[b : b + 1],
                    s_high[0:1],
                    s_low[0:1],
                    jnp.zeros((2, toks), F32),
                ],
                axis=0,
            )
            out[head, xi, toks:, :toks] = block.astype(BF16)


def cell_kernel(width, span, parts, aux, cell, normer, cell_out, normer_out, stabil_out, gated):
    toks = gated.shape[2]
    size = cell.shape[1]
    seqs = toks // span
    total = parts[0, 0].astype(F32)
    for xi in range(1, parts.shape[1]):
        total = total + parts[0, xi].astype(F32)
    rows = jnp.concatenate([total[toks:, :128], aux[0]], axis=0)
    cols = jnp.transpose(rows)[:toks]
    rows = rows[:, :toks]

    def small(get):
        scale = lax.rsqrt((get(4) + get(5)) / width + EPSILON)
        live = get(9) > 0.5
        gate_in = jnp.where(live, scale * (get(0) + get(1)), NEG_FILL)
        forget = scale * (get(2) + get(3)) + get(10)
        log_forget = jnp.minimum(forget, 0.0) - jnp.log1p(jnp.exp(-jnp.abs(forget)))
        return scale, live, gate_in, jnp.where(live, log_forget, 0.0), get(8)

    _, _, in_row, lf_row, m_row = small(lambda i: rows[i : i + 1])
    scale, live, in_col, lf_col, m_col = small(lambda i: cols[:, i : i + 1])
    at_row = lax.broadcasted_iota(jnp.int32, (toks, toks), 0)
    at_col = lax.broadcasted_iota(jnp.int32, (toks, toks), 1)
    same = (at_row // span) == (at_col // span)
    causal = same & (at_col <= at_row)
    anti = same & (at_row <= at_col)
    c_col = jnp.sum(jnp.where(causal, lf_row, 0.0), axis=1, keepdims=True)
    c_row = jnp.sum(jnp.where(anti, lf_col, 0.0), axis=0, keepdims=True)
    last_col = jnp.sum(jnp.where(same, lf_row, 0.0), axis=1, keepdims=True)
    last_row = jnp.sum(jnp.where(same, lf_col, 0.0), axis=0, keepdims=True)
    weight = jnp.where(causal, c_col - c_row + in_row, NEG_FILL)
    carried = c_col + m_col
    running = jnp.maximum(jnp.max(weight, axis=1, keepdims=True), carried)
    carry = jnp.exp(carried - running)

    def piece(i):
        return (scale * total[:toks, i * size : (i + 1) * size]).astype(BF16)

    query, key_vec, value, outgate = (piece(i) for i in range(4))
    shrink = size**-0.5
    scores = dot_nt(query, key_vec) * shrink * jnp.exp(weight - running)
    s_high, s_low = split_pair(scores)
    carried_out = []
    carried_norm = []
    query_wide = query.astype(F32)
    for r in range(seqs):
        at = slice(r * span, (r + 1) * span)
        high, low = split_pair(cell[r])
        carried_out.append(dot(query[at], high) + dot(query[at], low))
        carried_norm.append(jnp.sum(query_wide[at] * normer[0, r : r + 1], axis=1, keepdims=True))
    numer = dot(s_high, value) + dot(s_low, value) + carry * jnp.concatenate(carried_out, axis=0)
    denom = jnp.sum(scores, axis=1, keepdims=True) + carry * jnp.concatenate(carried_norm, axis=0)
    readout = jnp.where(live, numer / jnp.maximum(jnp.abs(denom), 1.0), 0.0)
    mixed = (readout * jax.nn.sigmoid(outgate.astype(F32))).astype(BF16)
    for xi in range(gated.shape[1]):
        gated[0, xi] = mixed

    top_col = jnp.maximum(
        jnp.max(jnp.where(same, last_col - c_row + in_row, NEG_FILL), axis=1, keepdims=True),
        last_col + m_col,
    )
    top_row = jnp.maximum(
        jnp.max(jnp.where(same, last_row - c_col + in_col, NEG_FILL), axis=0, keepdims=True),
        last_row + m_row,
    )
    source = jnp.exp(last_col - c_col + in_col - top_col)
    decay = jnp.exp(last_col + m_col - top_col)
    keyed = (key_vec.astype(F32) * shrink) * source
    k_high, k_low = split_pair(jnp.transpose(keyed))
    token_seq = lax.broadcasted_iota(jnp.int32, (toks, size), 0) // span
    for r in range(seqs):
        at = slice(r * span, (r + 1) * span)
        one = jnp.where(token_seq == r, value.astype(F32), 0.0).astype(BF16)
        fade = decay[r * span : r * span + 1]
        cell_out[r] = fade * cell[r] + (dot(k_high, one) + dot(k_low, one))
        normer_out[0, r : r + 1] = fade * normer[0, r : r + 1] + jnp.sum(
            keyed[at], axis=0, keepdims=True
        )
    stabil_out[0] = jnp.broadcast_to(top_row, (8, toks))


def mix_kernel(where, gated, *rest):
    weights, out = rest[:-1], rest[-1]
    y = where[0]
    ny = len(weights)
    cores, _, nx, toks, size = gated.shape
    for core in range(cores):
        total = None
        for k in range(ny):
            head = lax.rem(y + ny - k, ny)
            part = dot(gated[core, head].reshape(nx * toks, size), weights[k][...])
            total = part if total is None else total + part
        out[core] = total.astype(BF16).reshape(nx, toks, total.shape[1])


def add_kernel(parts, own, out, spread):
    total = parts[0].astype(F32)
    for i in range(1, parts.shape[0]):
        total = total + parts[i].astype(F32)
    done = (own[...].astype(F32) + total).astype(BF16)
    out[...] = done
    for i in range(spread.shape[0]):
        spread[i] = done


SMEM_SPEC = pl.BlockSpec(memory_space=pltpu.SMEM)
VMEM_SPEC = pl.BlockSpec(memory_space=pltpu.VMEM)


def per_device(
    tokens,
    lengths,
    norm_gain,
    query_weight,
    key_weight,
    value_weight,
    outgate_weight,
    input_gate_weight,
    forget_gate_weight,
    forget_bias,
    out_weight,
    cell_state,
    norm_state,
    max_state,
):
    seq_here, span, feat = tokens.shape
    layers, local_seqs, _, size, _ = cell_state.shape
    ny, nx, nc, nz = (lax.axis_size(a) for a in ("y", "x", "c", ZZ))
    toks = seq_here * span
    width = feat * nx * nc
    y, x, c = (lax.axis_index(a) for a in ("y", "x", "c"))
    z = lax.axis_index("zh") * lax.axis_size("zl") + lax.axis_index("zl")
    where = jnp.stack([y, c]).astype(jnp.int32)
    quarters = local_seqs // seq_here

    def shifted(array, step):
        return lax.ppermute(array, "y", [(i, (i + step) % ny) for i in range(ny)])

    def swapped(array):
        return lax.ppermute(array, "c", [(i, (i + 1) % nc) for i in range(nc)])

    def weights_of(layer):
        return jnp.concatenate(
            [w[layer] for w in (query_weight, key_weight, value_weight, outgate_weight)], axis=1
        )

    gains = lax.all_gather(norm_gain, "c", axis=0)
    live = jnp.arange(span, dtype=jnp.int32)[None, :] < lengths[:, None]

    def aux_of(layer):
        m = jnp.broadcast_to(max_state[layer], (local_seqs, span)).reshape(quarters, 1, toks)
        alive = live.astype(F32).reshape(quarters, 1, toks)
        bias = jnp.broadcast_to(forget_bias[layer, 0], (quarters, 1, toks))
        rows = jnp.concatenate([m, alive, bias, jnp.zeros((quarters, 5, toks), F32)], axis=1)
        return jnp.pad(rows, ((0, 0), (0, 0), (0, 128 - toks)))

    def gates_of(layer):
        cut = [
            lax.dynamic_slice(w[layer], (x * nc * feat, z * ny), (nc * feat, ny))
            for w in (input_gate_weight, forget_gate_weight)
        ]
        both = jnp.stack(cut, axis=2).reshape(nc, feat, 2 * ny)
        return jnp.transpose(both, (0, 2, 1))

    def gather_weights(joined):
        own = [joined] + [shifted(joined, k) for k in range(1, ny)]
        pairs = []
        for w in own:
            pairs += [w, swapped(w)]
        return pairs

    current = tokens.reshape(toks, feat)
    spread = jnp.broadcast_to(current[None], (nz, toks, feat))
    weights = gather_weights(weights_of(0))
    cells, normers, stabils = [], [], []
    for layer in range(layers):
        arrived = lax.all_to_all(spread, ZZ, 0, 0, tiled=True)
        halves = lax.all_to_all(
            arrived.reshape(nc, nx * toks, feat), "c", 0, 0, tiled=True
        ).reshape(nc, nx, toks, feat)
        parts = pl.pallas_call(
            project_kernel,
            out_shape=jax.ShapeDtypeStruct((ny, nx, toks + EXTRA, 4 * size), BF16),
            in_specs=[SMEM_SPEC] + [VMEM_SPEC] * (3 + 2 * ny),
            out_specs=VMEM_SPEC,
            name=f"project_{layer}",
        )(where, halves, gains[:, layer], gates_of(layer), *weights)
        summed = lax.all_to_all(
            parts.reshape(ny * nx, toks + EXTRA, 4 * size), YX, 0, 0, tiled=True
        ).reshape(ny, nx, toks + EXTRA, 4 * size)
        if layer == 0:
            own_out, summed = lax.optimization_barrier((out_weight[layer], summed))
            outs = [own_out] + [shifted(own_out, k) for k in range(1, ny)]
        cell_next, normer_next, top, gated = pl.pallas_call(
            lambda *refs: cell_kernel(width, span, *refs),
            grid=(quarters,),
            out_shape=(
                jax.ShapeDtypeStruct((local_seqs, size, size), F32),
                jax.ShapeDtypeStruct((quarters, seq_here, size), F32),
                jax.ShapeDtypeStruct((quarters, 8, toks), F32),
                jax.ShapeDtypeStruct((quarters, nx, toks, size), BF16),
            ),
            in_specs=[
                pl.BlockSpec((1, nx, toks + EXTRA, 4 * size), lambda i: (i, 0, 0, 0)),
                pl.BlockSpec((1, 8, 128), lambda i: (i, 0, 0)),
                pl.BlockSpec((seq_here, size, size), lambda i: (i, 0, 0)),
                pl.BlockSpec((1, seq_here, size), lambda i: (i, 0, 0)),
            ],
            out_specs=(
                pl.BlockSpec((seq_here, size, size), lambda i: (i, 0, 0)),
                pl.BlockSpec((1, seq_here, size), lambda i: (i, 0, 0)),
                pl.BlockSpec((1, 8, toks), lambda i: (i, 0, 0)),
                pl.BlockSpec((1, nx, toks, size), lambda i: (i, 0, 0, 0)),
            ),
            name=f"cell_{layer}",
        )(
            summed,
            aux_of(layer),
            cell_state[layer, :, 0],
            norm_state[layer, :, 0].reshape(quarters, seq_here, size),
        )
        cells.append(cell_next[:, None])
        normers.append(normer_next.reshape(local_seqs, 1, size))
        stabils.append(top[:, 0, ::span].reshape(local_seqs, 1))
        heads = lax.all_to_all(
            gated.reshape(quarters * nx, toks, size), YX, 0, 0, tiled=True
        ).reshape(ny, nx, toks, size)
        everyone = lax.all_gather(heads, "c", axis=0)
        mixed = pl.pallas_call(
            mix_kernel,
            out_shape=jax.ShapeDtypeStruct((nc, nx, toks, feat), BF16),
            in_specs=[SMEM_SPEC] + [VMEM_SPEC] * (1 + ny),
            out_specs=VMEM_SPEC,
            name=f"mix_{layer}",
        )(where, everyone, *outs)
        mixed = mixed.reshape(nz, toks, feat)
        if layer + 1 < layers:
            joined, mixed = lax.optimization_barrier(
                (jnp.concatenate([weights_of(layer + 1), out_weight[layer + 1]], axis=0), mixed)
            )
            moved = [joined] + [shifted(joined, k) for k in range(1, ny)]
            weights = []
            for w in moved:
                weights += [w[:feat], swapped(w[:feat])]
            outs = [w[feat:] for w in moved]
        added = lax.all_to_all(mixed, ZZ, 0, 0, tiled=True)
        current, spread = pl.pallas_call(
            add_kernel,
            out_shape=(
                jax.ShapeDtypeStruct((toks, feat), BF16),
                jax.ShapeDtypeStruct((nz, toks, feat), BF16),
            ),
            in_specs=[VMEM_SPEC] * 2,
            out_specs=(VMEM_SPEC, VMEM_SPEC),
            name=f"add_{layer}",
        )(added, current)
    return (
        current.reshape(seq_here, span, feat),
        jnp.stack(cells),
        jnp.stack(normers),
        jnp.stack(stabils),
    )


def solution(mesh):
    finer = Mesh(mesh.devices.reshape(4, 2, 4, 4, 2), ("zh", "zl", "y", "x", "c"))
    placed = (
        P(TP, None, DP),
        P(DP),
        P(None, DP),
        P(None, DP, TP),
        P(None, DP, TP),
        P(None, DP, TP),
        P(None, DP, TP),
        P(),
        P(),
        P(None, TP),
        P(None, TP, DP),
        P(None, DP, TP, None, None),
        P(None, DP, TP, None),
        P(None, DP, TP),
    )
    return jax.shard_map(
        per_device,
        mesh=finer,
        in_specs=placed,
        out_specs=(
            P(TP, None, DP),
            P(None, DP, TP, None, None),
            P(None, DP, TP, None),
            P(None, DP, TP),
        ),
        check_vma=False,
    )
```

time: 364 us -> 232 us (0.64)
  blocking collectives: 93.3 us -> 10.2 us
  waiting for transfers between devices: 152 us -> 80.2 us
  Pallas kernels: 0 us -> 31.6 us
  starting transfers between devices: 41 us -> 67.6 us
  matrix products: 21 us -> 0 us
  other arithmetic: 18.7 us -> 4.83 us
  between operations: 14.7 us -> 1.06 us
  local copies, waits for them, and re-layouts: 22.4 us -> 33.9 us
    all_gather x4 -> x0, waiting for transfers between devices: 100 us -> none  [whole_of(): whole = lax.all_gather(whole, axes[number], axis=dim, tiled=True)]
    all_to_all x2 -> x0, blocking collectives: 46.6 us -> none  [the longest x1 31.5 us: per_device(): lax.all_to_all(everyone, TP, split_axis=0, concat_axis=2, tiled=True)]
    all_gather x4 -> x3, blocking collectives: 46.6 us -> 10.2 us  [the longest x2 8.36 us: per_device(): everyone = lax.all_gather(heads, 'c', axis=0)]
    pallas_call x0 -> x8, Pallas kernels: none -> 31.6 us  [the longest x2 12.1 us: per_device(): pl.pallas_call(lambda *refs: cell_kernel(width, span, *refs), grid=(quart...]
    all_to_all x4 -> x10, waiting for transfers between devices: 35.3 us -> 62 us  [the longest x2 32.7 us: per_device(): lax.all_to_all(parts.reshape(ny * nx, toks + EXTRA, 4 * size), YX, 0, 0,...]
    dot_general x24 -> x0, matrix products: 21 us -> none  [the longest x10 9.12 us: partial_sum(): part = jnp.dot(scaled, weight, preferred_element_type=jnp.float32)]
    ppermute x0 -> x17, waiting for transfers between devices: none -> 18.2 us  [the longest x9 18.2 us: shifted(): return lax.ppermute(array, 'y', [(i, (i + step) % ny) for i in range(ny)])]
    ppermute x0 -> x17, starting transfers between devices: none -> 16.1 us  [the longest x9 10.2 us: shifted(): return lax.ppermute(array, 'y', [(i, (i + step) % ny) for i in range(ny)])]
  transfers between devices with their start and end apart: 10 -> 27, of which waited for: 10 -> 12; matrix products, arithmetic and copies ran while one was open for 8% -> 12% of each run, Pallas kernels for 0% -> 1%
where the time goes in v1:
time: 232 us; the launch traced here: 229 us
  waiting for transfers between devices  80.2 us (35%)
  starting transfers between devices  67.6 us (29%)
  local copies, waits for them, and re-layouts  33.9 us (15%)
  Pallas kernels  31.6 us (14%)
  blocking collectives  10.2 us (4%)
  other arithmetic  4.83 us (2%)
    all_to_all x2, waiting for transfers between devices, per_device(): lax.all_to_all(parts.reshape(ny * nx, toks + EXTRA, 4 * size), YX, 0, 0,...  32.7 us
    all_to_all x2, waiting for transfers between devices, per_device(): added = lax.all_to_all(mixed, ZZ, 0, 0, tiled=True)  20.4 us
    ppermute x9, waiting for transfers between devices, shifted(): return lax.ppermute(array, 'y', [(i, (i + step) % ny) for i in range(ny)])  18.2 us
    all_to_all x2, starting transfers between devices, per_device(): added = lax.all_to_all(mixed, ZZ, 0, 0, tiled=True)  13.3 us
    all_to_all x2, starting transfers between devices, per_device(): arrived = lax.all_to_all(spread, ZZ, 0, 0, tiled=True)  13 us
    pallas_call x2, Pallas kernels, per_device(): pl.pallas_call(lambda *refs: cell_kernel(width, span, *refs), grid=(quart...  12.1 us
    ppermute x9, starting transfers between devices, shifted(): return lax.ppermute(array, 'y', [(i, (i + step) % ny) for i in range(ny)])  10.2 us
    pallas_call x2, Pallas kernels, per_device(): pl.pallas_call(project_kernel, out_shape=jax.ShapeDtypeStruct((ny, nx, to...  10 us
  transfers between devices with their start and end apart: 27, of which 12 were waited for; matrix products, arithmetic and copies ran while one was open for 12% of the time, Pallas kernels for 1%

profile of v1, /device:TPU:1, one launch (start us, length us, event | category | flops | bytes accessed | tf_op | source)
XLA Modules:
  0.0 229.4 jit_solution(7172890679728865551)
XLA Ops:
  4.4 3.6 %collective-permute-start.5 = (bf16[512,512]{1,0:T(8,128)(2,1)S(1)}, bf16[512,512]{1,0:T(8,128)(2,1)S(1)}, u32[]{:S(2)}, u32[]{:S(2)}) collective-permute-start(bf16[512,512]{1,0:T(8,128)(2,1)S(1)} %pad_maximum_fusion.1.rest_0_), channel_id=1, source_target_pairs={{0,24},{8,0},{16,8},{24,16},{1,25},{9,1},{17,9},{25,17},{2,26},{10... | collective-permute-start | bytes 1572872 | tf_op jit(solution)/shard_map/ppermute | solution.py:215
  11.4 8.2 %all-to-all-start = ((bf16[8,64,512]{2,1,0:T(8,128)(2,1)}), bf16[8,64,512]{2,1,0:T(8,128)(2,1)}, u32[]{:S(2)}, u32[]{:S(2)}) async-start(bf16[8,64,512]{2,1,0:T(8,128)(2,1)} %broadcast_in_dim.34), calls=%async_computation | async-start | bytes 1048576 | tf_op jit(solution)/shard_map/all_to_all | solution.py:255
  25.0 4.7 %collective-permute-done.5.rest_6_ = bf16[512,512]{1,0:T(8,128)(2,1)S(1)} collective-permute-done((bf16[512,512]{1,0:T(8,128)(2,1)S(1)}, bf16[512,512]{1,0:T(8,128)(2,1)S(1)}, u32[]{:S(2)}, u32[]{:S(2)}) %collective-permute-start.5) | collective-permute-done | bytes 524320 | tf_op jit(solution)/shard_map/ppermute | solution.py:215
  31.5 3.2 %collective-permute-done.1.rest_2_ = bf16[512,512]{1,0:T(8,128)(2,1)S(1)} collective-permute-done((bf16[512,512]{1,0:T(8,128)(2,1)S(1)}, bf16[512,512]{1,0:T(8,128)(2,1)S(1)}, u32[]{:S(2)}, u32[]{:S(2)}) %collective-permute-start.1) | collective-permute-done | bytes 524320 | tf_op jit(solution)/shard_map/ppermute | solution.py:215
  39.9 3.6 %all-to-all-start.1 = ((bf16[2,256,512]{2,1,0:T(8,128)(2,1)}), bf16[2,256,512]{2,1,0:T(8,128)(2,1)S(1)}, u32[]{:S(2)}, u32[]{:S(2)}) async-start(bf16[2,256,512]{2,1,0:T(8,128)(2,1)} %bitcast.9), calls=%async_computation.1 | async-start | bytes 1048576 | tf_op jit(solution)/shard_map/all_to_all | solution.py:256
  45.9 5.0 %project_0.1 = bf16[4,4,72,512]{3,2,1,0:T(8,128)(2,1)} custom-call(s32[2]{0:T(128)} %pad_add_fusion.where, bf16[2,4,64,512]{3,2,1,0:T(8,128)(2,1)} %bitcast.93, f32[2,512]{1,0:T(2,128)} %bitcast.107, bf16[2,8,512]{2,1,0:T(8,128)(2,1)} %bitcast.103, bf16[512,512]{1,0:T(8,128)(2,1)} %copy-done.5, bf16[512,512]{1,0:T(8,128)(2,1)} %collective-permute-done.rest_1_, ...), custom_call_target="tpu_custom_call" | custom-call | tf_op jit(solution)/shard_map/project_0/pallas_call | solution.py:259
  50.9 4.3 %all-to-all-start.2 = ((bf16[16,72,512]{2,1,0:T(8,128)(2,1)}), bf16[16,72,512]{2,1,0:T(8,128)(2,1)S(1)}, u32[]{:S(2)}, u32[]{:S(2)}) async-start(bf16[16,72,512]{2,1,0:T(8,128)(2,1)} %bitcast.88), calls=%async_computation.2 | async-start | bytes 2359296 | tf_op jit(solution)/shard_map/all_to_all | solution.py:266
  59.0 14.2 %all-to-all-done.2 = bf16[16,72,512]{2,1,0:T(8,128)(2,1)S(1)} async-done(((bf16[16,72,512]{2,1,0:T(8,128)(2,1)}), bf16[16,72,512]{2,1,0:T(8,128)(2,1)S(1)}, u32[]{:S(2)}, u32[]{:S(2)}) %all-to-all-start.2) | async-done | bytes 1179680 | tf_op jit(solution)/shard_map/all_to_all | solution.py:266
  74.3 6.1 %cell_0.1 = (f32[16,128,128]{2,1,0:T(8,128)}, f32[4,4,128]{2,1,0:T(4,128)}, f32[4,8,64]{2,1,0:T(8,128)}, bf16[4,4,64,128]{3,2,1,0:T(8,128)(2,1)}) custom-call(bf16[4,4,72,512]{3,2,1,0:T(8,128)(2,1)} %bitcast.86, f32[4,8,128]{2,1,0:T(8,128)} %pad.7.refs_1_, f32[16,128,128]{2,1,0:T(8,128)} %get-tuple-element.53.refs_2_, f32[4,4,128]{2,1,0:T(4,128)} %bitcast.106), custom_call_target="tpu_custom_call" | custom-call | tf_op jit(solution)/shard_map/cell_0/pallas_call | solution.py:272
  80.3 4.8 %all-to-all-start.3 = ((bf16[16,64,128]{2,1,0:T(8,128)(2,1)}), bf16[16,64,128]{2,1,0:T(8,128)(2,1)S(1)}, u32[]{:S(2)}, u32[]{:S(2)}) async-start(bf16[16,64,128]{2,1,0:T(8,128)(2,1)} %bitcast.101), calls=%async_computation.3 | async-start | bytes 524288 | tf_op jit(solution)/shard_map/all_to_all | solution.py:303
  85.3 2.7 %collective-permute-start.9 = (bf16[128,512]{1,0:T(8,128)(2,1)S(1)}, bf16[128,512]{1,0:T(8,128)(2,1)S(1)}, u32[]{:S(2)}, u32[]{:S(2)}) collective-permute-start(bf16[128,512]{1,0:T(8,128)(2,1)S(1)} %get-tuple-element.21.rest_0_), channel_id=1, source_target_pairs={{0,24},{8,0},{16,8},{24,16},{1,25},{9,1},{17,9},{25,17},{2,26},{10... | collective-permute-start | bytes 393224 | tf_op jit(solution)/shard_map/ppermute | solution.py:215
  89.1 3.8 %all-to-all-done.3 = bf16[16,64,128]{2,1,0:T(8,128)(2,1)S(1)} async-done(((bf16[16,64,128]{2,1,0:T(8,128)(2,1)}), bf16[16,64,128]{2,1,0:T(8,128)(2,1)S(1)}, u32[]{:S(2)}, u32[]{:S(2)}) %all-to-all-start.3) | async-done | bytes 262176 | tf_op jit(solution)/shard_map/all_to_all | solution.py:303
  92.9 4.1 %all_gather.14.gated = bf16[2,4,4,64,128]{4,3,2,1,0:T(8,128)(2,1)} all-gather(bf16[1,4,4,64,128]{4,3,2,1,0:T(8,128)(2,1)S(1)} %bitcast.95), channel_id=1, replica_groups=mesh['zh'=4,'zl'=2,'y'=4,'x'=4,'c'=2] {'c'}, dimensions={0}, use_global_device_ids=true | all-gather | bytes 786432 | tf_op jit(solution)/shard_map/all_gather | solution.py:306
  97.0 2.0 collective-permute-done.7.rest_1_
  99.6 2.7 %mix_0.1 = bf16[2,4,64,512]{3,2,1,0:T(8,128)(2,1)} custom-call(s32[2]{0:T(128)} %pad_add_fusion.where, bf16[2,4,4,64,128]{4,3,2,1,0:T(8,128)(2,1)} %all_gather.14.gated, bf16[128,512]{1,0:T(8,128)(2,1)} %copy-done.18, bf16[128,512]{1,0:T(8,128)(2,1)} %copy-done.30, bf16[128,512]{1,0:T(8,128)(2,1)} %copy-done.29, bf16[128,512]{1,0:T(8,128)(2,1)} %copy-done.28), custom_call_target="tpu_custom_call" | custom-call | tf_op jit(solution)/shard_map/mix_0/pallas_call | solution.py:307
  102.4 8.1 %all-to-all-start.4 = ((bf16[8,64,512]{2,1,0:T(8,128)(2,1)}), bf16[8,64,512]{2,1,0:T(8,128)(2,1)S(1)}, u32[]{:S(2)}, u32[]{:S(2)}) async-start(bf16[8,64,512]{2,1,0:T(8,128)(2,1)} %bitcast.92), calls=%async_computation.4 | async-start | bytes 1048576 | tf_op jit(solution)/shard_map/all_to_all | solution.py:324
  112.2 12.5 %all-to-all-done.4.parts = bf16[8,64,512]{2,1,0:T(8,128)(2,1)S(1)} async-done(((bf16[8,64,512]{2,1,0:T(8,128)(2,1)}), bf16[8,64,512]{2,1,0:T(8,128)(2,1)S(1)}, u32[]{:S(2)}, u32[]{:S(2)}) %all-to-all-start.4) | async-done | bytes 524320 | tf_op jit(solution)/shard_map/all_to_all | solution.py:324
  125.5 2.0 add_0.1
  127.4 4.8 %all-to-all-start.5 = ((bf16[8,64,512]{2,1,0:T(8,128)(2,1)}), bf16[8,64,512]{2,1,0:T(8,128)(2,1)}, u32[]{:S(2)}, u32[]{:S(2)}) async-start(bf16[8,64,512]{2,1,0:T(8,128)(2,1)} %get-tuple-element.23), calls=%async_computation.5 | async-start | bytes 1048576 | tf_op jit(solution)/shard_map/all_to_all | solution.py:255
  135.3 8.3 %collective-permute-done.11 = bf16[640,512]{1,0:T(8,128)(2,1)} collective-permute-done((bf16[640,512]{1,0:T(8,128)(2,1)S(1)}, bf16[640,512]{1,0:T(8,128)(2,1)}, u32[]{:S(2)}, u32[]{:S(2)}) %collective-permute-start.11) | collective-permute-done | bytes 655392 | tf_op jit(solution)/shard_map/ppermute | solution.py:215
  146.6 4.9 %all-to-all-start.6 = ((bf16[2,256,512]{2,1,0:T(8,128)(2,1)}), bf16[2,256,512]{2,1,0:T(8,128)(2,1)S(1)}, u32[]{:S(2)}, u32[]{:S(2)}) async-start(bf16[2,256,512]{2,1,0:T(8,128)(2,1)} %bitcast.29), calls=%async_computation.6 | async-start | bytes 1048576 | tf_op jit(solution)/shard_map/all_to_all | solution.py:256
  153.7 5.0 %project_1.1 = bf16[4,4,72,512]{3,2,1,0:T(8,128)(2,1)} custom-call(s32[2]{0:T(128)} %pad_add_fusion.where, bf16[2,4,64,512]{3,2,1,0:T(8,128)(2,1)} %bitcast.94, f32[2,512]{1,0:T(2,128)} %bitcast.108, bf16[2,8,512]{2,1,0:T(8,128)(2,1)} %bitcast.104, bf16[512,512]{1,0:T(8,128)(2,1)} %copy-done.6, bf16[512,512]{1,0:T(8,128)(2,1)} %collective-permute-done.10.rest_1_, ...), custom_call_target="tpu_custom_call" | custom-call | tf_op jit(solution)/shard_map/project_1/pallas_call | solution.py:259
  158.7 3.7 %all-to-all-start.7 = ((bf16[16,72,512]{2,1,0:T(8,128)(2,1)}), bf16[16,72,512]{2,1,0:T(8,128)(2,1)S(1)}, u32[]{:S(2)}, u32[]{:S(2)}) async-start(bf16[16,72,512]{2,1,0:T(8,128)(2,1)} %bitcast.89), calls=%async_computation.7 | async-start | bytes 2359296 | tf_op jit(solution)/shard_map/all_to_all | solution.py:266
  163.0 18.5 %all-to-all-done.7 = bf16[16,72,512]{2,1,0:T(8,128)(2,1)S(1)} async-done(((bf16[16,72,512]{2,1,0:T(8,128)(2,1)}), bf16[16,72,512]{2,1,0:T(8,128)(2,1)S(1)}, u32[]{:S(2)}, u32[]{:S(2)}) %all-to-all-start.7) | async-done | bytes 1179680 | tf_op jit(solution)/shard_map/all_to_all | solution.py:266
  182.5 6.0 %cell_1.1 = (f32[16,128,128]{2,1,0:T(8,128)}, f32[4,4,128]{2,1,0:T(4,128)}, f32[4,8,64]{2,1,0:T(8,128)}, bf16[4,4,64,128]{3,2,1,0:T(8,128)(2,1)}) custom-call(bf16[4,4,72,512]{3,2,1,0:T(8,128)(2,1)} %bitcast.87, f32[4,8,128]{2,1,0:T(8,128)} %pad.8.refs_1_, f32[16,128,128]{2,1,0:T(8,128)} %get-tuple-element.52.refs_2_, f32[4,4,128]{2,1,0:T(4,128)} %bitcast.105), custom_call_target="tpu_custom_call" | custom-call | tf_op jit(solution)/shard_map/cell_1/pallas_call | solution.py:272
  188.6 3.8 %all-to-all-start.8 = ((bf16[16,64,128]{2,1,0:T(8,128)(2,1)}), bf16[16,64,128]{2,1,0:T(8,128)(2,1)S(1)}, u32[]{:S(2)}, u32[]{:S(2)}) async-start(bf16[16,64,128]{2,1,0:T(8,128)(2,1)} %bitcast.102), calls=%async_computation.8 | async-start | bytes 524288 | tf_op jit(solution)/shard_map/all_to_all | solution.py:303
  197.7 2.4 %all-to-all-done.8 = bf16[16,64,128]{2,1,0:T(8,128)(2,1)S(1)} async-done(((bf16[16,64,128]{2,1,0:T(8,128)(2,1)}), bf16[16,64,128]{2,1,0:T(8,128)(2,1)S(1)}, u32[]{:S(2)}, u32[]{:S(2)}) %all-to-all-start.8) | async-done | bytes 262176 | tf_op jit(solution)/shard_map/all_to_all | solution.py:303
  200.1 4.2 %all_gather.15.gated = bf16[2,4,4,64,128]{4,3,2,1,0:T(8,128)(2,1)} all-gather(bf16[1,4,4,64,128]{4,3,2,1,0:T(8,128)(2,1)S(1)} %bitcast.96), channel_id=1, replica_groups=mesh['zh'=4,'zl'=2,'y'=4,'x'=4,'c'=2] {'c'}, dimensions={0}, use_global_device_ids=true | all-gather | bytes 786432 | tf_op jit(solution)/shard_map/all_gather | solution.py:306
  204.3 2.9 %mix_1.1 = bf16[2,4,64,512]{3,2,1,0:T(8,128)(2,1)} custom-call(s32[2]{0:T(128)} %pad_add_fusion.where, bf16[2,4,4,64,128]{4,3,2,1,0:T(8,128)(2,1)} %all_gather.15.gated, bf16[128,512]{1,0:T(8,128)(2,1)} %slice.134.rest_0_, bf16[128,512]{1,0:T(8,128)(2,1)} %slice.147.rest_1_, bf16[128,512]{1,0:T(8,128)(2,1)} %slice.148.rest_2_, bf16[128,512]{1,0:T(8,128)(2,1)} %slice.149.rest_3_), custom_call_target="tpu_custom_call" | custom-call | tf_op jit(solution)/shard_map/mix_1/pallas_call | solution.py:307
  207.2 5.3 %all-to-all-start.9 = ((bf16[8,64,512]{2,1,0:T(8,128)(2,1)}), bf16[8,64,512]{2,1,0:T(8,128)(2,1)S(1)}, u32[]{:S(2)}, u32[]{:S(2)}) async-start(bf16[8,64,512]{2,1,0:T(8,128)(2,1)} %bitcast.91), calls=%async_computation.9 | async-start | bytes 1048576 | tf_op jit(solution)/shard_map/all_to_all | solution.py:324
  218.7 8.0 %all-to-all-done.9.parts = bf16[8,64,512]{2,1,0:T(8,128)(2,1)S(1)} async-done(((bf16[8,64,512]{2,1,0:T(8,128)(2,1)}), bf16[8,64,512]{2,1,0:T(8,128)(2,1)S(1)}, u32[]{:S(2)}, u32[]{:S(2)}) %all-to-all-start.9) | async-done | bytes 524320 | tf_op jit(solution)/shard_map/all_to_all | solution.py:324
  227.5 2.0 add_1.1
  (178 shorter events, 53.2 us)
Async XLA Ops:
  4.4 16.0 %copy-start.5 = (bf16[512,512]{1,0:T(8,128)(2,1)}, bf16[512,512]{1,0:T(8,128)(2,1)S(1)}, u32[]{:S(2)}) copy-start(bf16[512,512]{1,0:T(8,128)(2,1)S(1)} %pad_maximum_fusion.1.rest_0_) | copy-start | bytes 1572868
  4.4 25.3 %collective-permute-start.5 = (bf16[512,512]{1,0:T(8,128)(2,1)S(1)}, bf16[512,512]{1,0:T(8,128)(2,1)S(1)}, u32[]{:S(2)}, u32[]{:S(2)}) collective-permute-start(bf16[512,512]{1,0:T(8,128)(2,1)S(1)} %pad_maximum_fusion.1.rest_0_), channel_id=1, source_target_pairs={{0,24},{8,0},{16,8},{24,16},{1,25},{9,1},{17,9},{25,17},{2,26},{10... | collective-permute-start | bytes 1572872 | tf_op jit(solution)/shard_map/ppermute | solution.py:215
  8.0 23.4 %collective-permute-start.3 = (bf16[512,512]{1,0:T(8,128)(2,1)S(1)}, bf16[512,512]{1,0:T(8,128)(2,1)S(1)}, u32[]{:S(2)}, u32[]{:S(2)}) collective-permute-start(bf16[512,512]{1,0:T(8,128)(2,1)S(1)} %pad_maximum_fusion.1.rest_0_), channel_id=1, source_target_pairs={{0,16},{8,24},{16,0},{24,8},{1,17},{9,25},{17,1},{25,9},{2,18},{10... | collective-permute-start | bytes 1572872 | tf_op jit(solution)/shard_map/ppermute | solution.py:215
  8.4 26.3 %collective-permute-start.1 = (bf16[512,512]{1,0:T(8,128)(2,1)S(1)}, bf16[512,512]{1,0:T(8,128)(2,1)S(1)}, u32[]{:S(2)}, u32[]{:S(2)}) collective-permute-start(bf16[512,512]{1,0:T(8,128)(2,1)S(1)} %pad_maximum_fusion.1.rest_0_), channel_id=1, source_target_pairs={{0,8},{8,16},{16,24},{24,0},{1,9},{9,17},{17,25},{25,1},{2,10},{10... | collective-permute-start | bytes 1572872 | tf_op jit(solution)/shard_map/ppermute | solution.py:215
  9.1 34.5 %collective-permute-start = (bf16[512,512]{1,0:T(8,128)(2,1)S(1)}, bf16[512,512]{1,0:T(8,128)(2,1)}, u32[]{:S(2)}, u32[]{:S(2)}) collective-permute-start(bf16[512,512]{1,0:T(8,128)(2,1)S(1)} %pad_maximum_fusion.1.rest_0_), channel_id=1, source_target_pairs={{0,1},{1,0},{2,3},{3,2},{4,5},{5,4},{6,7},{7,6},{8,9},{9,8},{10,11... | collective-permute-start | bytes 1572872 | tf_op jit(solution)/shard_map/ppermute | solution.py:218
  11.4 28.5 %all-to-all-start = ((bf16[8,64,512]{2,1,0:T(8,128)(2,1)}), bf16[8,64,512]{2,1,0:T(8,128)(2,1)}, u32[]{:S(2)}, u32[]{:S(2)}) async-start(bf16[8,64,512]{2,1,0:T(8,128)(2,1)} %broadcast_in_dim.34), calls=%async_computation | async-start | bytes 1048576 | tf_op jit(solution)/shard_map/all_to_all | solution.py:255
  19.6 15.5 %copy-start.39 = (f32[2,16,1]{1,2,0:T(1,128)S(1)}, f32[2,16,1]{1,2,0:T(1,128)}, u32[]{:S(2)}) copy-start(f32[2,16,1]{1,2,0:T(1,128)} %param.27) | copy-start | bytes 388
  19.7 15.6 %copy-start.40 = (s32[16]{0:T(128)S(1)}, s32[16]{0:T(128)}, u32[]{:S(2)}) copy-start(s32[16]{0:T(128)} %param.15) | copy-start | bytes 196
  29.7 15.2 %collective-permute-start.6 = (bf16[512,512]{1,0:T(8,128)(2,1)S(1)}, bf16[512,512]{1,0:T(8,128)(2,1)S(1)}, u32[]{:S(2)}, u32[]{:S(2)}) collective-permute-start(bf16[512,512]{1,0:T(8,128)(2,1)S(1)} %collective-permute-done.5.rest_6_), channel_id=1, source_target_pairs={{0,1},{1,0},{2,3},{3,2},{4,5},{5,4},{6,7},{7,6},{8,9},{9,8},{10,11... | collective-permute-start | bytes 1572872 | tf_op jit(solution)/shard_map/ppermute | solution.py:218
  31.4 13.5 %collective-permute-start.4 = (bf16[512,512]{1,0:T(8,128)(2,1)S(1)}, bf16[512,512]{1,0:T(8,128)(2,1)}, u32[]{:S(2)}, u32[]{:S(2)}) collective-permute-start(bf16[512,512]{1,0:T(8,128)(2,1)S(1)} %collective-permute-done.3.rest_4_), channel_id=1, source_target_pairs={{0,1},{1,0},{2,3},{3,2},{4,5},{5,4},{6,7},{7,6},{8,9},{9,8},{10,11... | collective-permute-start | bytes 1572872 | tf_op jit(solution)/shard_map/ppermute | solution.py:218
  34.7 10.2 %collective-permute-start.2 = (bf16[512,512]{1,0:T(8,128)(2,1)S(1)}, bf16[512,512]{1,0:T(8,128)(2,1)}, u32[]{:S(2)}, u32[]{:S(2)}) collective-permute-start(bf16[512,512]{1,0:T(8,128)(2,1)S(1)} %collective-permute-done.1.rest_2_), channel_id=1, source_target_pairs={{0,1},{1,0},{2,3},{3,2},{4,5},{5,4},{6,7},{7,6},{8,9},{9,8},{10,11... | collective-permute-start | bytes 1572872 | tf_op jit(solution)/shard_map/ppermute | solution.py:218
  39.9 5.0 %all-to-all-start.1 = ((bf16[2,256,512]{2,1,0:T(8,128)(2,1)}), bf16[2,256,512]{2,1,0:T(8,128)(2,1)S(1)}, u32[]{:S(2)}, u32[]{:S(2)}) async-start(bf16[2,256,512]{2,1,0:T(8,128)(2,1)} %bitcast.9), calls=%async_computation.1 | async-start | bytes 1048576 | tf_op jit(solution)/shard_map/all_to_all | solution.py:256
  50.9 22.3 %all-to-all-start.2 = ((bf16[16,72,512]{2,1,0:T(8,128)(2,1)}), bf16[16,72,512]{2,1,0:T(8,128)(2,1)S(1)}, u32[]{:S(2)}, u32[]{:S(2)}) async-start(bf16[16,72,512]{2,1,0:T(8,128)(2,1)} %bitcast.88), calls=%async_computation.2 | async-start | bytes 2359296 | tf_op jit(solution)/shard_map/all_to_all | solution.py:266
  57.6 30.9 %copy-start.18 = (bf16[128,512]{1,0:T(8,128)(2,1)}, bf16[128,512]{1,0:T(8,128)(2,1)S(1)}, u32[]{:S(2)}) copy-start(bf16[128,512]{1,0:T(8,128)(2,1)S(1)} %get-tuple-element.21.rest_0_) | copy-start | bytes 393220
  80.3 12.5 %all-to-all-start.3 = ((bf16[16,64,128]{2,1,0:T(8,128)(2,1)}), bf16[16,64,128]{2,1,0:T(8,128)(2,1)S(1)}, u32[]{:S(2)}, u32[]{:S(2)}) async-start(bf16[16,64,128]{2,1,0:T(8,128)(2,1)} %bitcast.101), calls=%async_computation.3 | async-start | bytes 524288 | tf_op jit(solution)/shard_map/all_to_all | solution.py:303
  85.3 11.7 %collective-permute-start.9 = (bf16[128,512]{1,0:T(8,128)(2,1)S(1)}, bf16[128,512]{1,0:T(8,128)(2,1)S(1)}, u32[]{:S(2)}, u32[]{:S(2)}) collective-permute-start(bf16[128,512]{1,0:T(8,128)(2,1)S(1)} %get-tuple-element.21.rest_0_), channel_id=1, source_target_pairs={{0,24},{8,0},{16,8},{24,16},{1,25},{9,1},{17,9},{25,17},{2,26},{10... | collective-permute-start | bytes 393224 | tf_op jit(solution)/shard_map/ppermute | solution.py:215
  87.9 9.1 %collective-permute-start.8 = (bf16[128,512]{1,0:T(8,128)(2,1)S(1)}, bf16[128,512]{1,0:T(8,128)(2,1)S(1)}, u32[]{:S(2)}, u32[]{:S(2)}) collective-permute-start(bf16[128,512]{1,0:T(8,128)(2,1)S(1)} %get-tuple-element.21.rest_0_), channel_id=1, source_target_pairs={{0,16},{8,24},{16,0},{24,8},{1,17},{9,25},{17,1},{25,9},{2,18},{10... | collective-permute-start | bytes 393224 | tf_op jit(solution)/shard_map/ppermute | solution.py:215
  88.5 10.5 %collective-permute-start.7 = (bf16[128,512]{1,0:T(8,128)(2,1)S(1)}, bf16[128,512]{1,0:T(8,128)(2,1)S(1)}, u32[]{:S(2)}, u32[]{:S(2)}) collective-permute-start(bf16[128,512]{1,0:T(8,128)(2,1)S(1)} %get-tuple-element.21.rest_0_), channel_id=1, source_target_pairs={{0,8},{8,16},{16,24},{24,0},{1,9},{9,17},{17,25},{25,1},{2,10},{10... | collective-permute-start | bytes 393224 | tf_op jit(solution)/shard_map/ppermute | solution.py:215
  102.4 22.3 %all-to-all-start.4 = ((bf16[8,64,512]{2,1,0:T(8,128)(2,1)}), bf16[8,64,512]{2,1,0:T(8,128)(2,1)S(1)}, u32[]{:S(2)}, u32[]{:S(2)}) async-start(bf16[8,64,512]{2,1,0:T(8,128)(2,1)} %bitcast.92), calls=%async_computation.4 | async-start | bytes 1048576 | tf_op jit(solution)/shard_map/all_to_all | solution.py:324
  110.5 23.2 %collective-permute-start.15 = (bf16[640,512]{1,0:T(8,128)(2,1)S(1)}, bf16[640,512]{1,0:T(8,128)(2,1)S(1)}, u32[]{:S(2)}, u32[]{:S(2)}) collective-permute-start(bf16[640,512]{1,0:T(8,128)(2,1)S(1)} %pad_maximum_fusion), channel_id=1, source_target_pairs={{0,24},{8,0},{16,8},{24,16},{1,25},{9,1},{17,9},{25,17},{2,26},{10... | collective-permute-start | bytes 1966088 | tf_op jit(solution)/shard_map/ppermute | solution.py:215
  111.3 23.1 %collective-permute-start.13 = (bf16[640,512]{1,0:T(8,128)(2,1)S(1)}, bf16[640,512]{1,0:T(8,128)(2,1)S(1)}, u32[]{:S(2)}, u32[]{:S(2)}) collective-permute-start(bf16[640,512]{1,0:T(8,128)(2,1)S(1)} %pad_maximum_fusion), channel_id=1, source_target_pairs={{0,16},{8,24},{16,0},{24,8},{1,17},{9,25},{17,1},{25,9},{2,18},{10... | collective-permute-start | bytes 1966088 | tf_op jit(solution)/shard_map/ppermute | solution.py:215
  111.3 32.3 %collective-permute-start.11 = (bf16[640,512]{1,0:T(8,128)(2,1)S(1)}, bf16[640,512]{1,0:T(8,128)(2,1)}, u32[]{:S(2)}, u32[]{:S(2)}) collective-permute-start(bf16[640,512]{1,0:T(8,128)(2,1)S(1)} %pad_maximum_fusion), channel_id=1, source_target_pairs={{0,8},{8,16},{16,24},{24,0},{1,9},{9,17},{17,25},{25,1},{2,10},{10... | collective-permute-start | bytes 1966088 | tf_op jit(solution)/shard_map/ppermute | solution.py:215
  127.4 19.2 %all-to-all-start.5 = ((bf16[8,64,512]{2,1,0:T(8,128)(2,1)}), bf16[8,64,512]{2,1,0:T(8,128)(2,1)}, u32[]{:S(2)}, u32[]{:S(2)}) async-start(bf16[8,64,512]{2,1,0:T(8,128)(2,1)} %get-tuple-element.23), calls=%async_computation.5 | async-start | bytes 1048576 | tf_op jit(solution)/shard_map/all_to_all | solution.py:255
  132.2 19.3 %collective-permute-start.10 = (bf16[512,512]{1,0:T(8,128)(2,1)S(1)}, bf16[512,512]{1,0:T(8,128)(2,1)}, u32[]{:S(2)}, u32[]{:S(2)}) collective-permute-start(bf16[512,512]{1,0:T(8,128)(2,1)S(1)} %slice.126.rest_0_), channel_id=1, source_target_pairs={{0,1},{1,0},{2,3},{3,2},{4,5},{5,4},{6,7},{7,6},{8,9},{9,8},{10,11... | collective-permute-start | bytes 1572872 | tf_op jit(solution)/shard_map/ppermute | solution.py:218
  133.7 17.8 %collective-permute-start.16 = (bf16[512,512]{1,0:T(8,128)(2,1)S(1)}, bf16[512,512]{1,0:T(8,128)(2,1)}, u32[]{:S(2)}, u32[]{:S(2)}) collective-permute-start(bf16[512,512]{1,0:T(8,128)(2,1)S(1)} %slice.145.rest_6_), channel_id=1, source_target_pairs={{0,1},{1,0},{2,3},{3,2},{4,5},{5,4},{6,7},{7,6},{8,9},{9,8},{10,11... | collective-permute-start | bytes 1572872 | tf_op jit(solution)/shard_map/ppermute | solution.py:218
  134.5 18.4 %copy-start.8 = (bf16[512,512]{1,0:T(8,128)(2,1)}, bf16[512,512]{1,0:T(8,128)(2,1)S(1)}, u32[]{:S(2)}) copy-start(bf16[512,512]{1,0:T(8,128)(2,1)S(1)} %slice.144.rest_4_) | copy-start | bytes 1572868
  134.5 17.0 %collective-permute-start.14 = (bf16[512,512]{1,0:T(8,128)(2,1)S(1)}, bf16[512,512]{1,0:T(8,128)(2,1)}, u32[]{:S(2)}, u32[]{:S(2)}) collective-permute-start(bf16[512,512]{1,0:T(8,128)(2,1)S(1)} %slice.144.rest_4_), channel_id=1, source_target_pairs={{0,1},{1,0},{2,3},{3,2},{4,5},{5,4},{6,7},{7,6},{8,9},{9,8},{10,11... | collective-permute-start | bytes 1572872 | tf_op jit(solution)/shard_map/ppermute | solution.py:218
  144.7 6.8 %collective-permute-start.12 = (bf16[512,512]{1,0:T(8,128)(2,1)S(1)}, bf16[512,512]{1,0:T(8,128)(2,1)}, u32[]{:S(2)}, u32[]{:S(2)}) collective-permute-start(bf16[512,512]{1,0:T(8,128)(2,1)S(1)} %slice.143.rest_2_), channel_id=1, source_target_pairs={{0,1},{1,0},{2,3},{3,2},{4,5},{5,4},{6,7},{7,6},{8,9},{9,8},{10,11... | collective-permute-start | bytes 1572872 | tf_op jit(solution)/shard_map/ppermute | solution.py:218
  146.6 6.3 %all-to-all-start.6 = ((bf16[2,256,512]{2,1,0:T(8,128)(2,1)}), bf16[2,256,512]{2,1,0:T(8,128)(2,1)S(1)}, u32[]{:S(2)}, u32[]{:S(2)}) async-start(bf16[2,256,512]{2,1,0:T(8,128)(2,1)} %bitcast.29), calls=%async_computation.6 | async-start | bytes 1048576 | tf_op jit(solution)/shard_map/all_to_all | solution.py:256
  158.7 22.8 %all-to-all-start.7 = ((bf16[16,72,512]{2,1,0:T(8,128)(2,1)}), bf16[16,72,512]{2,1,0:T(8,128)(2,1)S(1)}, u32[]{:S(2)}, u32[]{:S(2)}) async-start(bf16[16,72,512]{2,1,0:T(8,128)(2,1)} %bitcast.89), calls=%async_computation.7 | async-start | bytes 2359296 | tf_op jit(solution)/shard_map/all_to_all | solution.py:266
  188.6 11.5 %all-to-all-start.8 = ((bf16[16,64,128]{2,1,0:T(8,128)(2,1)}), bf16[16,64,128]{2,1,0:T(8,128)(2,1)S(1)}, u32[]{:S(2)}, u32[]{:S(2)}) async-start(bf16[16,64,128]{2,1,0:T(8,128)(2,1)} %bitcast.102), calls=%async_computation.8 | async-start | bytes 524288 | tf_op jit(solution)/shard_map/all_to_all | solution.py:303
  207.2 19.5 %all-to-all-start.9 = ((bf16[8,64,512]{2,1,0:T(8,128)(2,1)}), bf16[8,64,512]{2,1,0:T(8,128)(2,1)S(1)}, u32[]{:S(2)}, u32[]{:S(2)}) async-start(bf16[8,64,512]{2,1,0:T(8,128)(2,1)} %bitcast.91), calls=%async_computation.9 | async-start | bytes 1048576 | tf_op jit(solution)/shard_map/all_to_all | solution.py:324
  (36 other events, 264.3 us)

commit v2 on v1

--- a/solution.py
+++ b/solution.py
@@ -31,15 +31,15 @@
     return lax.dot_general(a, b, (((1,), (1,)), ((), ())), preferred_element_type=F32)
 
 
-def project_kernel(where, tokens, gain, gates, *rest):
+def project_kernel(where, tokens, swapped, gain, gates, *rest):
     weights, out = rest[:-1], rest[-1]
     y, c = where[0], where[1]
     ny = len(weights) // 2
     nx, toks, feat = tokens.shape[1:]
     halves = []
     squares = []
-    for half in (c, 1 - c):
-        wide = tokens[half].reshape(nx * toks, feat).astype(F32)
+    for source, half in ((tokens, c), (swapped, 1 - c)):
+        wide = source[c].reshape(nx * toks, feat).astype(F32)
         halves.append((wide * gain[pl.ds(half, 1), :]).astype(BF16))
         squares.append(split_pair(wide * wide))
     gate_half = [gates[c], gates[1 - c]]
@@ -52,7 +52,7 @@
         extras.append((both, square))
     for k in range(ny):
         head = lax.rem(y + ny - k, ny)
-        done = dot(halves[0], weights[2 * k][...]) + dot(halves[1], weights[2 * k + 1][...])
+        done = dot(halves[0], weights[2 * k][:feat]) + dot(halves[1], weights[2 * k + 1][:feat])
         out[head, :, :toks, :] = done.astype(BF16).reshape(nx, toks, done.shape[1])
     out[:, :, toks:, :] = jnp.zeros((ny, nx, EXTRA, out.shape[3]), BF16)
     for xi in range(nx):
@@ -166,7 +166,7 @@
         total = None
         for k in range(ny):
             head = lax.rem(y + ny - k, ny)
-            part = dot(gated[core, head].reshape(nx * toks, size), weights[k][...])
+            part = dot(gated[core, head].reshape(nx * toks, size), weights[k][-size:])
             total = part if total is None else total + part
         out[core] = total.astype(BF16).reshape(nx, toks, total.shape[1])
 
@@ -181,8 +181,21 @@
         spread[i] = done
 
 
+def pack_kernel(query, key_vec, value, outgate, last, joined, *spread):
+    size = query.shape[2]
+    feat = query.shape[1]
+    for i, source in enumerate((query, key_vec, value, outgate)):
+        joined[:feat, i * size : (i + 1) * size] = source[0]
+    for copies in spread:
+        for i in range(copies.shape[0]):
+            copies[i] = last[...]
+    if not spread:
+        joined[feat:] = last[0]
+
+
 SMEM_SPEC = pl.BlockSpec(memory_space=pltpu.SMEM)
 VMEM_SPEC = pl.BlockSpec(memory_space=pltpu.VMEM)
+HBM_SPEC = pl.BlockSpec(memory_space=pltpu.HBM)
 
 
 def per_device(
@@ -217,11 +230,6 @@
     def swapped(array):
         return lax.ppermute(array, "c", [(i, (i + 1) % nc) for i in range(nc)])
 
-    def weights_of(layer):
-        return jnp.concatenate(
-            [w[layer] for w in (query_weight, key_weight, value_weight, outgate_weight)], axis=1
-        )
-
     gains = lax.all_gather(norm_gain, "c", axis=0)
     live = jnp.arange(span, dtype=jnp.int32)[None, :] < lengths[:, None]
 
@@ -240,88 +248,121 @@
         both = jnp.stack(cut, axis=2).reshape(nc, feat, 2 * ny)
         return jnp.transpose(both, (0, 2, 1))
 
-    def gather_weights(joined):
-        own = [joined] + [shifted(joined, k) for k in range(1, ny)]
-        pairs = []
-        for w in own:
-            pairs += [w, swapped(w)]
-        return pairs
-
+    projections = (query_weight, key_weight, value_weight, outgate_weight)
     current = tokens.reshape(toks, feat)
-    spread = jnp.broadcast_to(current[None], (nz, toks, feat))
-    weights = gather_weights(weights_of(0))
-    cells, normers, stabils = [], [], []
+
+    def pack(layer, last, last_spec, out_shape):
+        whole = [pl.BlockSpec(o.shape, lambda i, n=len(o.shape): (0,) * n) for o in out_shape]
+        return pl.pallas_call(
+            pack_kernel,
+            grid=(1,),
+            out_shape=out_shape,
+            in_specs=[pl.BlockSpec((1, feat, size), lambda i: (layer, 0, 0))] * 4 + [last_spec],
+            out_specs=whole,
+            compiler_params=pltpu.CompilerParams(vmem_limit_bytes=60 << 20),
+        )(*projections, last)
+
+    joined, spread = pack(
+        0,
+        current,
+        pl.BlockSpec((toks, feat), lambda i: (0, 0)),
+        [
+            jax.ShapeDtypeStruct((feat, 4 * size), BF16),
+            jax.ShapeDtypeStruct((nz, toks, feat), BF16),
+        ],
+    )
+    spread = spread.reshape(nz * toks, feat)
+    moved = [joined] + [shifted(joined, k) for k in range(1, ny)]
+    own_out, moved[ny // 2] = lax.optimization_barrier((out_weight[0], moved[ny // 2]))
+    outs = [own_out] + [shifted(own_out, k) for k in range(1, ny)]
+    weights = []
+    for w in moved:
+        weights += [w, swapped(w)]
+    states = []
     for layer in range(layers):
         arrived = lax.all_to_all(spread, ZZ, 0, 0, tiled=True)
-        halves = lax.all_to_all(
-            arrived.reshape(nc, nx * toks, feat), "c", 0, 0, tiled=True
-        ).reshape(nc, nx, toks, feat)
+        if layer == 0:
+            (packed,) = pack(
+                1,
+                out_weight,
+                pl.BlockSpec((1, size, feat), lambda i: (1, 0, 0)),
+                [jax.ShapeDtypeStruct((feat + size, 4 * size), BF16)],
+            )
+            auxes = [aux_of(n) for n in range(layers)]
+            gates = [gates_of(n) for n in range(layers)]
+            gains = [gains[:, n] for n in range(layers)]
+            (arrived, auxes, gates, gains, where, packed) = lax.optimization_barrier(
+                (arrived, auxes, gates, gains, where, packed)
+            )
+        other = swapped(arrived).reshape(nc, nx, toks, feat)
+        arrived = arrived.reshape(nc, nx, toks, feat)
         parts = pl.pallas_call(
             project_kernel,
             out_shape=jax.ShapeDtypeStruct((ny, nx, toks + EXTRA, 4 * size), BF16),
-            in_specs=[SMEM_SPEC] + [VMEM_SPEC] * (3 + 2 * ny),
+            in_specs=[SMEM_SPEC] + [VMEM_SPEC] * (4 + 2 * ny),
             out_specs=VMEM_SPEC,
-            name=f"project_{layer}",
-        )(where, halves, gains[:, layer], gates_of(layer), *weights)
+            compiler_params=pltpu.CompilerParams(vmem_limit_bytes=16 << 20),
+        )(where, arrived, other, gains[layer], gates[layer], *weights)
         summed = lax.all_to_all(
-            parts.reshape(ny * nx, toks + EXTRA, 4 * size), YX, 0, 0, tiled=True
+            parts.reshape(ny * nx * (toks + EXTRA), 4 * size), YX, 0, 0, tiled=True
         ).reshape(ny, nx, toks + EXTRA, 4 * size)
-        if layer == 0:
-            own_out, summed = lax.optimization_barrier((out_weight[layer], summed))
-            outs = [own_out] + [shifted(own_out, k) for k in range(1, ny)]
-        cell_next, normer_next, top, gated = pl.pallas_call(
-            lambda *refs: cell_kernel(width, span, *refs),
+        first = layer * quarters
+        state_specs = (
+            pl.BlockSpec((seq_here, size, size), lambda i: (first + i, 0, 0)),
+            pl.BlockSpec((1, seq_here, size), lambda i: (first + i, 0, 0)),
+            pl.BlockSpec((1, 8, toks), lambda i: (first + i, 0, 0)),
+        )
+        kept = [HBM_SPEC] * len(states)
+        *states, gated = pl.pallas_call(
+            lambda *refs: cell_kernel(width, span, *refs[:4], *refs[4 + len(kept) :]),
             grid=(quarters,),
             out_shape=(
-                jax.ShapeDtypeStruct((local_seqs, size, size), F32),
-                jax.ShapeDtypeStruct((quarters, seq_here, size), F32),
-                jax.ShapeDtypeStruct((quarters, 8, toks), F32),
+                jax.ShapeDtypeStruct((layers * local_seqs, size, size), F32),
+                jax.ShapeDtypeStruct((layers * quarters, seq_here, size), F32),
+                jax.ShapeDtypeStruct((layers * quarters, 8, toks), F32),
                 jax.ShapeDtypeStruct((quarters, nx, toks, size), BF16),
             ),
             in_specs=[
                 pl.BlockSpec((1, nx, toks + EXTRA, 4 * size), lambda i: (i, 0, 0, 0)),
                 pl.BlockSpec((1, 8, 128), lambda i: (i, 0, 0)),
-                pl.BlockSpec((seq_here, size, size), lambda i: (i, 0, 0)),
-                pl.BlockSpec((1, seq_here, size), lambda i: (i, 0, 0)),
+                *state_specs[:2],
+                *kept,
             ],
             out_specs=(
-                pl.BlockSpec((seq_here, size, size), lambda i: (i, 0, 0)),
-                pl.BlockSpec((1, seq_here, size), lambda i: (i, 0, 0)),
-                pl.BlockSpec((1, 8, toks), lambda i: (i, 0, 0)),
+                *state_specs,
                 pl.BlockSpec((1, nx, toks, size), lambda i: (i, 0, 0, 0)),
             ),
-            name=f"cell_{layer}",
+            input_output_aliases={4 + n: n for n in range(len(kept))},
+            compiler_params=pltpu.CompilerParams(vmem_limit_bytes=10 << 20),
         )(
             summed,
-            aux_of(layer),
-            cell_state[layer, :, 0],
-            norm_state[layer, :, 0].reshape(quarters, seq_here, size),
+            auxes[layer],
+            cell_state.reshape(layers * local_seqs, size, size),
+            norm_state.reshape(layers * quarters, seq_here, size),
+            *states,
         )
-        cells.append(cell_next[:, None])
-        normers.append(normer_next.reshape(local_seqs, 1, size))
-        stabils.append(top[:, 0, ::span].reshape(local_seqs, 1))
+        if layer + 1 < layers:
+            packed, gated = lax.optimization_barrier((packed, gated))
         heads = lax.all_to_all(
-            gated.reshape(quarters * nx, toks, size), YX, 0, 0, tiled=True
+            gated.reshape(quarters * nx * toks, size), YX, 0, 0, tiled=True
         ).reshape(ny, nx, toks, size)
+        if layer + 1 < layers:
+            moved = [packed] + [shifted(packed, k) for k in range(1, ny)]
+            weights = []
+            for w in moved:
+                weights += [w, swapped(w)]
+            next_outs = moved
         everyone = lax.all_gather(heads, "c", axis=0)
         mixed = pl.pallas_call(
             mix_kernel,
             out_shape=jax.ShapeDtypeStruct((nc, nx, toks, feat), BF16),
             in_specs=[SMEM_SPEC] + [VMEM_SPEC] * (1 + ny),
             out_specs=VMEM_SPEC,
-            name=f"mix_{layer}",
+            compiler_params=pltpu.CompilerParams(vmem_limit_bytes=8 << 20),
         )(where, everyone, *outs)
-        mixed = mixed.reshape(nz, toks, feat)
-        if layer + 1 < layers:
-            joined, mixed = lax.optimization_barrier(
-                (jnp.concatenate([weights_of(layer + 1), out_weight[layer + 1]], axis=0), mixed)
-            )
-            moved = [joined] + [shifted(joined, k) for k in range(1, ny)]
-            weights = []
-            for w in moved:
-                weights += [w[:feat], swapped(w[:feat])]
-            outs = [w[feat:] for w in moved]
-        added = lax.all_to_all(mixed, ZZ, 0, 0, tiled=True)
+        mixed = mixed.reshape(nz * toks, feat)
+        added = lax.all_to_all(mixed, ZZ, 0, 0, tiled=True).reshape(nz, toks, feat)
+        outs = next_outs
         current, spread = pl.pallas_call(
             add_kernel,
             out_shape=(
@@ -330,13 +371,15 @@
             ),
             in_specs=[VMEM_SPEC] * 2,
             out_specs=(VMEM_SPEC, VMEM_SPEC),
-            name=f"add_{layer}",
+            compiler_params=pltpu.CompilerParams(vmem_limit_bytes=8 << 20),
         )(added, current)
+        spread = spread.reshape(nz * toks, feat)
+    cell_next, normer_next, top = states
     return (
         current.reshape(seq_here, span, feat),
-        jnp.stack(cells),
-        jnp.stack(normers),
-        jnp.stack(stabils),
+        cell_next.reshape(cell_state.shape),
+        normer_next.reshape(norm_state.shape),
+        top[:, 0, ::span].reshape(max_state.shape),
     )
 
 
@@ -358,6 +401,7 @@
         P(None, DP, TP, None),
         P(None, DP, TP),
     )
+
     return jax.shard_map(
         per_device,
         mesh=finer,

time: 232 us -> 221 us (0.953)
  blocking collectives: 10.2 us -> 86.1 us
  waiting for transfers between devices: 80.2 us -> 35.4 us
  local copies, waits for them, and re-layouts: 33.9 us -> 9.12 us
  starting transfers between devices: 67.6 us -> 60.1 us
  Pallas kernels: 31.6 us -> 26.7 us
  other arithmetic: 4.83 us -> 0.85 us
    all_to_all x0 -> x4, blocking collectives: none -> 75.6 us  [the longest x2 44.5 us: per_device(): lax.all_to_all(parts.reshape(ny * nx * (toks + EXTRA), 4 * size), YX, 0,...]
    all_to_all x8 -> x2, waiting for transfers between devices: 62 us -> 15.6 us  [the longest x1 12.3 us: per_device(): added = lax.all_to_all(mixed, ZZ, 0, 0, tiled=True).reshape(nz, toks, feat)]
    all_to_all x8 -> x2, starting transfers between devices: 38.5 us -> 9.92 us  [the longest x1 6.39 us: per_device(): added = lax.all_to_all(mixed, ZZ, 0, 0, tiled=True).reshape(nz, toks, feat)]
    ppermute x8 -> x10, starting transfers between devices: 5.91 us -> 22.6 us  [swapped(): return lax.ppermute(array, 'c', [(i, (i + 1) % nc) for i in range(nc)])]
    slice x13 -> x3, local copies, waits for them, and re-layouts: 9.83 us -> 0.61 us  [the longest x2 0.6 us: per_device(): top[:, 0, ::span].reshape(max_state.shape)]
    unnamed x84 -> x28, local copies, waits for them, and re-layouts: 8.66 us -> 1.74 us
    ppermute x9, waiting for transfers between devices: 18.2 us -> 12.8 us  [shifted(): return lax.ppermute(array, 'y', [(i, (i + step) % ny) for i in range(ny)])]
    ppermute x8 -> x10, waiting for transfers between devices: 0.02 us -> 5.13 us  [swapped(): return lax.ppermute(array, 'c', [(i, (i + 1) % nc) for i in range(nc)])]
  transfers between devices with their start and end apart: 27 -> 23, of which waited for: 12 -> 11; matrix products, arithmetic and copies ran while one was open for 12% -> 4% of each run, Pallas kernels for 1% -> 1%
where the time goes in v2:
time: 221 us; the launch traced here: 219 us
  blocking collectives  86.1 us (39%)
  starting transfers between devices  60.1 us (27%)
  waiting for transfers between devices  35.4 us (16%)
  Pallas kernels  26.7 us (12%)
  local copies, waits for them, and re-layouts  9.12 us (4%)
    all_to_all x2, blocking collectives, per_device(): lax.all_to_all(parts.reshape(ny * nx * (toks + EXTRA), 4 * size), YX, 0,...  44.5 us
    ppermute x10, starting transfers between devices, swapped(): return lax.ppermute(array, 'c', [(i, (i + 1) % nc) for i in range(nc)])  22.6 us
    all_to_all x1, blocking collectives, per_device(): added = lax.all_to_all(mixed, ZZ, 0, 0, tiled=True).reshape(nz, toks, feat)  20.3 us
    ppermute x9, starting transfers between devices, shifted(): return lax.ppermute(array, 'y', [(i, (i + step) % ny) for i in range(ny)])  13.8 us
    all_to_all x2, starting transfers between devices, per_device(): arrived = lax.all_to_all(spread, ZZ, 0, 0, tiled=True)  13.8 us
    ppermute x9, waiting for transfers between devices, shifted(): return lax.ppermute(array, 'y', [(i, (i + step) % ny) for i in range(ny)])  12.8 us
    all_to_all x1, waiting for transfers between devices, per_device(): added = lax.all_to_all(mixed, ZZ, 0, 0, tiled=True).reshape(nz, toks, feat)  12.3 us
    all_to_all x1, blocking collectives, per_device(): lax.all_to_all(gated.reshape(quarters * nx * toks, size), YX, 0, 0, tiled...  10.8 us
  transfers between devices with their start and end apart: 23, of which 11 were waited for; matrix products, arithmetic and copies ran while one was open for 4% of the time, Pallas kernels for 1%

profile of v2, /device:TPU:1, one launch (start us, length us, event | category | flops | bytes accessed | tf_op | source)
XLA Modules:
  0.0 219.2 jit_solution(5816662940017156327)
XLA Ops:
  0.6 2.2 %shard_map.165 = (bf16[512,512]{1,0:T(8,128)(2,1)}, bf16[8,64,512]{2,1,0:T(8,128)(2,1)}) custom-call(bf16[2,512,128]{2,1,0:T(8,128)(2,1)} %query.3, bf16[2,512,128]{2,1,0:T(8,128)(2,1)} %key_vec.3, bf16[2,512,128]{2,1,0:T(8,128)(2,1)} %value.3, bf16[2,512,128]{2,1,0:T(8,128)(2,1)} %outgate.3, bf16[64,512]{1,0:T(8,128)(2,1)} %bitcast.71), custom_call_target="tpu_custom_call" | custom-call | tf_op jit(solution)/shard_map/pallas_call | solution.py:256
  2.9 3.7 %collective-permute-start.4 = (bf16[512,512]{1,0:T(8,128)(2,1)}, bf16[512,512]{1,0:T(8,128)(2,1)S(1)}, u32[]{:S(2)}, u32[]{:S(2)}) collective-permute-start(bf16[512,512]{1,0:T(8,128)(2,1)} %get-tuple-element.36.rest_0_), channel_id=1, source_target_pairs={{0,16},{8,24},{16,0},{24,8},{1,17},{9,25},{17,1},{25,9},{2,18},{10... | collective-permute-start | bytes 1572872 | tf_op jit(solution)/shard_map/ppermute | solution.py:228
  7.0 2.3 %collective-permute-start.6 = (bf16[512,512]{1,0:T(8,128)(2,1)}, bf16[512,512]{1,0:T(8,128)(2,1)S(1)}, u32[]{:S(2)}, u32[]{:S(2)}) collective-permute-start(bf16[512,512]{1,0:T(8,128)(2,1)} %get-tuple-element.36.rest_0_), channel_id=1, source_target_pairs={{0,24},{8,0},{16,8},{24,16},{1,25},{9,1},{17,9},{25,17},{2,26},{10... | collective-permute-start | bytes 1572872 | tf_op jit(solution)/shard_map/ppermute | solution.py:228
  9.3 1.5 collective-permute-start.1
  10.8 8.2 %all-to-all-start = ((bf16[8,64,512]{2,1,0:T(8,128)(2,1)}), bf16[8,64,512]{2,1,0:T(8,128)(2,1)S(1)}, u32[]{:S(2)}, u32[]{:S(2)}) async-start(bf16[8,64,512]{2,1,0:T(8,128)(2,1)} %get-tuple-element.30), calls=%async_computation | async-start | bytes 1048576 | tf_op jit(solution)/shard_map/all_to_all | solution.py:283
  24.2 2.2 shard_map.166.rest_0_
  26.4 1.8 all-gather.1
  31.3 1.9 all-to-all-done
  33.3 1.4 collective-permute-start
  34.7 1.5 collective-permute-done
  36.3 3.0 %shard_map.167 = bf16[4,4,72,512]{3,2,1,0:T(8,128)(2,1)S(1)} custom-call(s32[2]{0:T(128)S(1)} %pad_add_fusion.where, bf16[2,4,64,512]{3,2,1,0:T(8,128)(2,1)S(1)} %bitcast.67, bf16[2,4,64,512]{3,2,1,0:T(8,128)(2,1)S(1)} %bitcast.69, f32[2,512]{1,0:T(2,128)S(1)} %get-tuple-element.34.gain, bf16[2,8,512]{2,1,0:T(8,128)(2,1)S(1)} %bitcast.77, ...), custom_call_target="tpu_custom_call" | custom-call | tf_op jit(solution)/shard_map/pallas_call | solution.py:299
  39.3 22.1 %all_to_all.72 = bf16[16,72,512]{2,1,0:T(8,128)(2,1)S(1)} all-to-all(bf16[16,72,512]{2,1,0:T(8,128)(2,1)S(1)} %bitcast.64), channel_id=1, replica_groups=mesh['zh'=4,'zl'=2,'y'=4,'x'=4,'c'=2] {'y','x'}, dimensions={0} | all-to-all | bytes 2359296 | tf_op jit(solution)/shard_map/all_to_all | solution.py:306
  61.4 4.8 %shard_map.168 = (f32[32,128,128]{2,1,0:T(8,128)}, f32[8,4,128]{2,1,0:T(4,128)}, f32[8,8,64]{2,1,0:T(8,128)S(1)}, bf16[4,4,64,128]{3,2,1,0:T(8,128)(2,1)}) custom-call(bf16[4,4,72,512]{3,2,1,0:T(8,128)(2,1)S(1)} %bitcast.63, f32[4,8,128]{2,1,0:T(8,128)S(1)} %pad.7.refs_1_, f32[32,128,128]{2,1,0:T(8,128)S(1)} %bitcast.60, f32[8,4,128]{2,1,0:T(4,128)S(1)} %bitcast.74), custom_call_target="tpu_custom_call" | custom-call | tf_op jit(solution)/shard_map/pallas_call | solution.py:316
  66.2 3.5 %all-to-all-start.2 = ((bf16[16,64,128]{2,1,0:T(8,128)(2,1)}), bf16[16,64,128]{2,1,0:T(8,128)(2,1)S(1)}, u32[]{:S(2)}, u32[]{:S(2)}) async-start(bf16[16,64,128]{2,1,0:T(8,128)(2,1)} %bitcast.22), calls=%async_computation.2 | async-start | bytes 524288 | tf_op jit(solution)/shard_map/all_to_all | solution.py:346
  69.7 2.5 %collective-permute-start.10 = (bf16[128,512]{1,0:T(8,128)(2,1)S(1)}, bf16[128,512]{1,0:T(8,128)(2,1)S(1)}, u32[]{:S(2)}, u32[]{:S(2)}) collective-permute-start(bf16[128,512]{1,0:T(8,128)(2,1)S(1)} %slice_bitcast_fusion.rest_0_), channel_id=1, source_target_pairs={{0,24},{8,0},{16,8},{24,16},{1,25},{9,1},{17,9},{25,17},{2,26},{10... | collective-permute-start | bytes 393224 | tf_op jit(solution)/shard_map/ppermute | solution.py:228
  72.3 1.7 collective-permute-start.9
  74.0 3.2 %all-to-all-done.2 = bf16[16,64,128]{2,1,0:T(8,128)(2,1)S(1)} async-done(((bf16[16,64,128]{2,1,0:T(8,128)(2,1)}), bf16[16,64,128]{2,1,0:T(8,128)(2,1)S(1)}, u32[]{:S(2)}, u32[]{:S(2)}) %all-to-all-start.2) | async-done | bytes 262176 | tf_op jit(solution)/shard_map/all_to_all | solution.py:346
  77.3 4.5 %all_gather.14.gated = bf16[2,4,4,64,128]{4,3,2,1,0:T(8,128)(2,1)S(1)} all-gather(bf16[1,4,4,64,128]{4,3,2,1,0:T(8,128)(2,1)S(1)} %bitcast.79), channel_id=1, replica_groups=mesh['zh'=4,'zl'=2,'y'=4,'x'=4,'c'=2] {'c'}, dimensions={0}, use_global_device_ids=true | all-gather | bytes 786432 | tf_op jit(solution)/shard_map/all_gather | solution.py:355
  83.6 20.3 %all_to_all.73.parts = bf16[8,64,512]{2,1,0:T(8,128)(2,1)S(1)} all-to-all(bf16[8,64,512]{2,1,0:T(8,128)(2,1)S(1)} %bitcast.68), channel_id=1, replica_groups=mesh['zh'=4,'zl'=2,'y'=4,'x'=4,'c'=2] {'zl','zh'}, dimensions={0} | all-to-all | bytes 1048576 | tf_op jit(solution)/shard_map/all_to_all | solution.py:364
  104.9 5.6 %all-to-all-start.4 = ((bf16[8,64,512]{2,1,0:T(8,128)(2,1)}), bf16[8,64,512]{2,1,0:T(8,128)(2,1)}, u32[]{:S(2)}, u32[]{:S(2)}) async-start(bf16[8,64,512]{2,1,0:T(8,128)(2,1)} %get-tuple-element.42), calls=%async_computation.4 | async-start | bytes 1048576 | tf_op jit(solution)/shard_map/all_to_all | solution.py:283
  111.7 2.0 collective-permute-start.17
  113.6 2.9 %collective-permute-start.12 = (bf16[640,512]{1,0:T(8,128)(2,1)S(1)}, bf16[640,512]{1,0:T(8,128)(2,1)}, u32[]{:S(2)}, u32[]{:S(2)}) collective-permute-start(bf16[640,512]{1,0:T(8,128)(2,1)S(1)} %copy-done.1), channel_id=1, source_target_pairs={{0,1},{1,0},{2,3},{3,2},{4,5},{5,4},{6,7},{7,6},{8,9},{9,8},{10,11... | collective-permute-start | bytes 1966088 | tf_op jit(solution)/shard_map/ppermute | solution.py:231
  116.5 11.9 %collective-permute-done.13.rest_2_.rest_1_ = bf16[640,512]{1,0:T(8,128)(2,1)S(1)} collective-permute-done((bf16[640,512]{1,0:T(8,128)(2,1)S(1)}, bf16[640,512]{1,0:T(8,128)(2,1)S(1)}, u32[]{:S(2)}, u32[]{:S(2)}) %collective-permute-start.13) | collective-permute-done | bytes 655392 | tf_op jit(solution)/shard_map/ppermute | solution.py:228
  128.3 14.8 %collective-permute-start.14 = (bf16[640,512]{1,0:T(8,128)(2,1)S(1)}, bf16[640,512]{1,0:T(8,128)(2,1)}, u32[]{:S(2)}, u32[]{:S(2)}) collective-permute-start(bf16[640,512]{1,0:T(8,128)(2,1)S(1)} %collective-permute-done.13.rest_2_.rest_1_), channel_id=1, source_target_pairs={{0,1},{1,0},{2,3},{3,2},{4,5},{5,4},{6,7},{7,6},{8,9},{9,8},{10,11... | collective-permute-start | bytes 1966088 | tf_op jit(solution)/shard_map/ppermute | solution.py:231
  148.8 3.9 %shard_map.171 = bf16[4,4,72,512]{3,2,1,0:T(8,128)(2,1)S(1)} custom-call(s32[2]{0:T(128)S(1)} %copy-done.7, bf16[2,4,64,512]{3,2,1,0:T(8,128)(2,1)} %bitcast.25.tokens, bf16[2,4,64,512]{3,2,1,0:T(8,128)(2,1)S(1)} %bitcast.70, f32[2,512]{1,0:T(2,128)S(1)} %copy-done.5, bf16[2,8,512]{2,1,0:T(8,128)(2,1)S(1)} %bitcast.76, bf16[640,512]{1,0:T(8,128)(2,1)S(1)} %copy-done.1, ...), custom_call_target="tpu_custom_call" | custom-call | tf_op jit(solution)/shard_map/pallas_call | solution.py:299
  152.7 22.4 %all_to_all.74 = bf16[16,72,512]{2,1,0:T(8,128)(2,1)S(1)} all-to-all(bf16[16,72,512]{2,1,0:T(8,128)(2,1)S(1)} %bitcast.62), channel_id=1, replica_groups=mesh['zh'=4,'zl'=2,'y'=4,'x'=4,'c'=2] {'y','x'}, dimensions={0} | all-to-all | bytes 2359296 | tf_op jit(solution)/shard_map/all_to_all | solution.py:306
  175.1 4.7 %shard_map.172 = (f32[32,128,128]{2,1,0:T(8,128)}, f32[8,4,128]{2,1,0:T(4,128)}, f32[8,8,64]{2,1,0:T(8,128)S(1)}, bf16[4,4,64,128]{3,2,1,0:T(8,128)(2,1)S(1)}) custom-call(bf16[4,4,72,512]{3,2,1,0:T(8,128)(2,1)S(1)} %bitcast.65, f32[4,8,128]{2,1,0:T(8,128)S(1)} %pad.8.refs_1_, ...), custom_call_target="tpu_custom_call", output_to_operand_aliasing={{0}: (4, {}), {1}: (5, {}), {2}: (6, {})} | custom-call | tf_op jit(solution)/shard_map/pallas_call | solution.py:316
  179.8 10.8 %all_to_all.75 = bf16[16,64,128]{2,1,0:T(8,128)(2,1)S(1)} all-to-all(bf16[16,64,128]{2,1,0:T(8,128)(2,1)S(1)} %bitcast.73), channel_id=1, replica_groups=mesh['zh'=4,'zl'=2,'y'=4,'x'=4,'c'=2] {'y','x'}, dimensions={0} | all-to-all | bytes 524288 | tf_op jit(solution)/shard_map/all_to_all | solution.py:346
  190.6 4.2 %all_gather.15.gated = bf16[2,4,4,64,128]{4,3,2,1,0:T(8,128)(2,1)S(1)} all-gather(bf16[1,4,4,64,128]{4,3,2,1,0:T(8,128)(2,1)S(1)} %bitcast.80), channel_id=1, replica_groups=mesh['zh'=4,'zl'=2,'y'=4,'x'=4,'c'=2] {'c'}, dimensions={0}, use_global_device_ids=true | all-gather | bytes 786432 | tf_op jit(solution)/shard_map/all_gather | solution.py:355
  194.9 2.8 %shard_map.173 = bf16[2,4,64,512]{3,2,1,0:T(8,128)(2,1)} custom-call(s32[2]{0:T(128)S(1)} %copy-done.7, bf16[2,4,4,64,128]{4,3,2,1,0:T(8,128)(2,1)S(1)} %all_gather.15.gated, bf16[640,512]{1,0:T(8,128)(2,1)S(1)} %copy-done.1, bf16[640,512]{1,0:T(8,128)(2,1)S(1)} %collective-permute-done.13.rest_2_.rest_1_, ...), custom_call_target="tpu_custom_call" | custom-call | tf_op jit(solution)/shard_map/pallas_call | solution.py:356
  197.6 6.4 %all-to-all-start.7 = ((bf16[8,64,512]{2,1,0:T(8,128)(2,1)}), bf16[8,64,512]{2,1,0:T(8,128)(2,1)S(1)}, u32[]{:S(2)}, u32[]{:S(2)}) async-start(bf16[8,64,512]{2,1,0:T(8,128)(2,1)} %bitcast.32), calls=%async_computation.7 | async-start | bytes 1048576 | tf_op jit(solution)/shard_map/all_to_all | solution.py:364
  205.9 12.3 %all-to-all-done.7.parts = bf16[8,64,512]{2,1,0:T(8,128)(2,1)S(1)} async-done(((bf16[8,64,512]{2,1,0:T(8,128)(2,1)}), bf16[8,64,512]{2,1,0:T(8,128)(2,1)S(1)}, u32[]{:S(2)}, u32[]{:S(2)}) %all-to-all-start.7) | async-done | bytes 524320 | tf_op jit(solution)/shard_map/all_to_all | solution.py:364
  (100 shorter events, 21.2 us)
Async XLA Ops:
  0.6 18.3 %copy-start.8 = (bf16[2,4096,32]{1,2,0:T(8,128)(2,1)S(1)}, bf16[2,4096,32]{1,2,0:T(8,128)(2,1)}, u32[]{:S(2)}) copy-start(bf16[2,4096,32]{1,2,0:T(8,128)(2,1)} %param.22) | copy-start | bytes 1572868
  2.9 26.9 %collective-permute-start.4 = (bf16[512,512]{1,0:T(8,128)(2,1)}, bf16[512,512]{1,0:T(8,128)(2,1)S(1)}, u32[]{:S(2)}, u32[]{:S(2)}) collective-permute-start(bf16[512,512]{1,0:T(8,128)(2,1)} %get-tuple-element.36.rest_0_), channel_id=1, source_target_pairs={{0,16},{8,24},{16,0},{24,8},{1,17},{9,25},{17,1},{25,9},{2,18},{10... | collective-permute-start | bytes 1572872 | tf_op jit(solution)/shard_map/ppermute | solution.py:228
  6.6 23.8 %collective-permute-start.2 = (bf16[512,512]{1,0:T(8,128)(2,1)}, bf16[512,512]{1,0:T(8,128)(2,1)S(1)}, u32[]{:S(2)}, u32[]{:S(2)}) collective-permute-start(bf16[512,512]{1,0:T(8,128)(2,1)} %get-tuple-element.36.rest_0_), channel_id=1, source_target_pairs={{0,8},{8,16},{16,24},{24,0},{1,9},{9,17},{17,25},{25,1},{2,10},{10... | collective-permute-start | bytes 1572872 | tf_op jit(solution)/shard_map/ppermute | solution.py:228
  7.0 23.9 %collective-permute-start.6 = (bf16[512,512]{1,0:T(8,128)(2,1)}, bf16[512,512]{1,0:T(8,128)(2,1)S(1)}, u32[]{:S(2)}, u32[]{:S(2)}) collective-permute-start(bf16[512,512]{1,0:T(8,128)(2,1)} %get-tuple-element.36.rest_0_), channel_id=1, source_target_pairs={{0,24},{8,0},{16,8},{24,16},{1,25},{9,1},{17,9},{25,17},{2,26},{10... | collective-permute-start | bytes 1572872 | tf_op jit(solution)/shard_map/ppermute | solution.py:228
  9.3 25.5 %collective-permute-start.1 = (bf16[512,512]{1,0:T(8,128)(2,1)}, bf16[512,512]{1,0:T(8,128)(2,1)S(1)}, u32[]{:S(2)}, u32[]{:S(2)}) collective-permute-start(bf16[512,512]{1,0:T(8,128)(2,1)} %get-tuple-element.36.rest_0_), channel_id=1, source_target_pairs={{0,1},{1,0},{2,3},{3,2},{4,5},{5,4},{6,7},{7,6},{8,9},{9,8},{10,11... | collective-permute-start | bytes 1572872 | tf_op jit(solution)/shard_map/ppermute | solution.py:231
  10.8 22.5 %all-to-all-start = ((bf16[8,64,512]{2,1,0:T(8,128)(2,1)}), bf16[8,64,512]{2,1,0:T(8,128)(2,1)S(1)}, u32[]{:S(2)}, u32[]{:S(2)}) async-start(bf16[8,64,512]{2,1,0:T(8,128)(2,1)} %get-tuple-element.30), calls=%async_computation | async-start | bytes 1048576 | tf_op jit(solution)/shard_map/all_to_all | solution.py:283
  19.0 4.7 %copy-start.13 = (s32[16]{0:T(128)S(1)}, s32[16]{0:T(128)}, u32[]{:S(2)}) copy-start(s32[16]{0:T(128)} %param.15) | copy-start | bytes 196
  21.1 5.2 %copy-start.10 = (f32[2,512]{1,0:T(2,128)S(1)}, f32[2,512]{1,0:T(2,128)}, u32[]{:S(2)}) copy-start(f32[2,512]{1,0:T(2,128)} %param.16) | copy-start | bytes 12292
  24.2 12.1 %copy-start.2 = (bf16[512,512]{1,0:T(8,128)(2,1)S(1)}, bf16[512,512]{1,0:T(8,128)(2,1)}, u32[]{:S(2)}) copy-start(bf16[512,512]{1,0:T(8,128)(2,1)} %get-tuple-element.36.rest_0_) | copy-start | bytes 1572868
  28.3 54.1 %copy-start.6 = (s32[2]{0:T(128)}, s32[2]{0:T(128)S(1)}, u32[]{:S(2)}) copy-start(s32[2]{0:T(128)S(1)} %pad_add_fusion.where) | copy-start | bytes 28
  29.8 4.9 %collective-permute-start.5 = (bf16[512,512]{1,0:T(8,128)(2,1)S(1)}, bf16[512,512]{1,0:T(8,128)(2,1)}, u32[]{:S(2)}, u32[]{:S(2)}) collective-permute-start(bf16[512,512]{1,0:T(8,128)(2,1)S(1)} %collective-permute-done.4.rest_4_), channel_id=1, source_target_pairs={{0,1},{1,0},{2,3},{3,2},{4,5},{5,4},{6,7},{7,6},{8,9},{9,8},{10,11... | collective-permute-start | bytes 1572872 | tf_op jit(solution)/shard_map/ppermute | solution.py:231
  30.4 4.3 %collective-permute-start.3 = (bf16[512,512]{1,0:T(8,128)(2,1)S(1)}, bf16[512,512]{1,0:T(8,128)(2,1)}, u32[]{:S(2)}, u32[]{:S(2)}) collective-permute-start(bf16[512,512]{1,0:T(8,128)(2,1)S(1)} %collective-permute-done.2.rest_2_), channel_id=1, source_target_pairs={{0,1},{1,0},{2,3},{3,2},{4,5},{5,4},{6,7},{7,6},{8,9},{9,8},{10,11... | collective-permute-start | bytes 1572872 | tf_op jit(solution)/shard_map/ppermute | solution.py:231
  30.9 3.8 %collective-permute-start.7 = (bf16[512,512]{1,0:T(8,128)(2,1)S(1)}, bf16[512,512]{1,0:T(8,128)(2,1)}, u32[]{:S(2)}, u32[]{:S(2)}) collective-permute-start(bf16[512,512]{1,0:T(8,128)(2,1)S(1)} %collective-permute-done.6.rest_6_), channel_id=1, source_target_pairs={{0,1},{1,0},{2,3},{3,2},{4,5},{5,4},{6,7},{7,6},{8,9},{9,8},{10,11... | collective-permute-start | bytes 1572872 | tf_op jit(solution)/shard_map/ppermute | solution.py:231
  33.3 3.0 %collective-permute-start = (bf16[512,512]{1,0:T(8,128)(2,1)S(1)}, bf16[512,512]{1,0:T(8,128)(2,1)S(1)}, u32[]{:S(2)}, u32[]{:S(2)}) collective-permute-start(bf16[512,512]{1,0:T(8,128)(2,1)S(1)} %bitcast.66), channel_id=1, source_target_pairs={{0,1},{1,0},{2,3},{3,2},{4,5},{5,4},{6,7},{7,6},{8,9},{9,8},{10,11... | collective-permute-start | bytes 1572872 | tf_op jit(solution)/shard_map/ppermute | solution.py:231
  39.3 22.1 %copy-start = (f32[2,16,1,128,128]{4,3,2,1,0:T(8,128)S(1)}, f32[2,16,1,128,128]{4,3,2,1,0:T(8,128)}, u32[]{:S(2)}) copy-start(f32[2,16,1,128,128]{4,3,2,1,0:T(8,128)} %param.25) | copy-start | bytes 6291460
  39.3 22.1 %copy-start.4 = (f32[2,16,1,128]{3,2,1,0:T(1,128)S(1)}, f32[2,16,1,128]{3,2,1,0:T(1,128)}, u32[]{:S(2)}) copy-start(f32[2,16,1,128]{3,2,1,0:T(1,128)} %param.26) | copy-start | bytes 49156
  66.2 11.0 %all-to-all-start.2 = ((bf16[16,64,128]{2,1,0:T(8,128)(2,1)}), bf16[16,64,128]{2,1,0:T(8,128)(2,1)S(1)}, u32[]{:S(2)}, u32[]{:S(2)}) async-start(bf16[16,64,128]{2,1,0:T(8,128)(2,1)} %bitcast.22), calls=%async_computation.2 | async-start | bytes 524288 | tf_op jit(solution)/shard_map/all_to_all | solution.py:346
  69.7 12.0 %collective-permute-start.10 = (bf16[128,512]{1,0:T(8,128)(2,1)S(1)}, bf16[128,512]{1,0:T(8,128)(2,1)S(1)}, u32[]{:S(2)}, u32[]{:S(2)}) collective-permute-start(bf16[128,512]{1,0:T(8,128)(2,1)S(1)} %slice_bitcast_fusion.rest_0_), channel_id=1, source_target_pairs={{0,24},{8,0},{16,8},{24,16},{1,25},{9,1},{17,9},{25,17},{2,26},{10... | collective-permute-start | bytes 393224 | tf_op jit(solution)/shard_map/ppermute | solution.py:228
  72.3 9.4 %collective-permute-start.8 = (bf16[128,512]{1,0:T(8,128)(2,1)S(1)}, bf16[128,512]{1,0:T(8,128)(2,1)S(1)}, u32[]{:S(2)}, u32[]{:S(2)}) collective-permute-start(bf16[128,512]{1,0:T(8,128)(2,1)S(1)} %slice_bitcast_fusion.rest_0_), channel_id=1, source_target_pairs={{0,8},{8,16},{16,24},{24,0},{1,9},{9,17},{17,25},{25,1},{2,10},{10... | collective-permute-start | bytes 393224 | tf_op jit(solution)/shard_map/ppermute | solution.py:228
  72.3 10.1 %collective-permute-start.9 = (bf16[128,512]{1,0:T(8,128)(2,1)S(1)}, bf16[128,512]{1,0:T(8,128)(2,1)S(1)}, u32[]{:S(2)}, u32[]{:S(2)}) collective-permute-start(bf16[128,512]{1,0:T(8,128)(2,1)S(1)} %slice_bitcast_fusion.rest_0_), channel_id=1, source_target_pairs={{0,16},{8,24},{16,0},{24,8},{1,17},{9,25},{17,1},{25,9},{2,18},{10... | collective-permute-start | bytes 393224 | tf_op jit(solution)/shard_map/ppermute | solution.py:228
  81.7 22.2 %copy-start.3 = (bf16[4,16,512]{2,1,0:T(8,128)(2,1)S(1)}, bf16[4,16,512]{2,1,0:T(8,128)(2,1)}, u32[]{:S(2)}) copy-start(bf16[4,16,512]{2,1,0:T(8,128)(2,1)} %param.14) | copy-start | bytes 196612
  83.6 26.9 %copy-start.1 = (bf16[640,512]{1,0:T(8,128)(2,1)S(1)}, bf16[640,512]{1,0:T(8,128)(2,1)}, u32[]{:S(2)}) copy-start(bf16[640,512]{1,0:T(8,128)(2,1)} %shard_map.166.rest_0_) | copy-start | bytes 1966084
  104.9 39.0 %all-to-all-start.4 = ((bf16[8,64,512]{2,1,0:T(8,128)(2,1)}), bf16[8,64,512]{2,1,0:T(8,128)(2,1)}, u32[]{:S(2)}, u32[]{:S(2)}) async-start(bf16[8,64,512]{2,1,0:T(8,128)(2,1)} %get-tuple-element.42), calls=%async_computation.4 | async-start | bytes 1048576 | tf_op jit(solution)/shard_map/all_to_all | solution.py:283
  110.5 17.9 %collective-permute-start.13 = (bf16[640,512]{1,0:T(8,128)(2,1)S(1)}, bf16[640,512]{1,0:T(8,128)(2,1)S(1)}, u32[]{:S(2)}, u32[]{:S(2)}) collective-permute-start(bf16[640,512]{1,0:T(8,128)(2,1)S(1)} %copy-done.1), channel_id=1, source_target_pairs={{0,8},{8,16},{16,24},{24,0},{1,9},{9,17},{17,25},{25,1},{2,10},{10... | collective-permute-start | bytes 1966088 | tf_op jit(solution)/shard_map/ppermute | solution.py:228
  110.7 32.4 %collective-permute-start.15 = (bf16[640,512]{1,0:T(8,128)(2,1)S(1)}, bf16[640,512]{1,0:T(8,128)(2,1)}, u32[]{:S(2)}, u32[]{:S(2)}) collective-permute-start(bf16[640,512]{1,0:T(8,128)(2,1)S(1)} %copy-done.1), channel_id=1, source_target_pairs={{0,16},{8,24},{16,0},{24,8},{1,17},{9,25},{17,1},{25,9},{2,18},{10... | collective-permute-start | bytes 1966088 | tf_op jit(solution)/shard_map/ppermute | solution.py:228
  111.7 31.5 %collective-permute-start.17 = (bf16[640,512]{1,0:T(8,128)(2,1)S(1)}, bf16[640,512]{1,0:T(8,128)(2,1)}, u32[]{:S(2)}, u32[]{:S(2)}) collective-permute-start(bf16[640,512]{1,0:T(8,128)(2,1)S(1)} %copy-done.1), channel_id=1, source_target_pairs={{0,24},{8,0},{16,8},{24,16},{1,25},{9,1},{17,9},{25,17},{2,26},{10... | collective-permute-start | bytes 1966088 | tf_op jit(solution)/shard_map/ppermute | solution.py:228
  113.6 30.2 %collective-permute-start.12 = (bf16[640,512]{1,0:T(8,128)(2,1)S(1)}, bf16[640,512]{1,0:T(8,128)(2,1)}, u32[]{:S(2)}, u32[]{:S(2)}) collective-permute-start(bf16[640,512]{1,0:T(8,128)(2,1)S(1)} %copy-done.1), channel_id=1, source_target_pairs={{0,1},{1,0},{2,3},{3,2},{4,5},{5,4},{6,7},{7,6},{8,9},{9,8},{10,11... | collective-permute-start | bytes 1966088 | tf_op jit(solution)/shard_map/ppermute | solution.py:231
  128.3 16.6 %collective-permute-start.14 = (bf16[640,512]{1,0:T(8,128)(2,1)S(1)}, bf16[640,512]{1,0:T(8,128)(2,1)}, u32[]{:S(2)}, u32[]{:S(2)}) collective-permute-start(bf16[640,512]{1,0:T(8,128)(2,1)S(1)} %collective-permute-done.13.rest_2_.rest_1_), channel_id=1, source_target_pairs={{0,1},{1,0},{2,3},{3,2},{4,5},{5,4},{6,7},{7,6},{8,9},{9,8},{10,11... | collective-permute-start | bytes 1966088 | tf_op jit(solution)/shard_map/ppermute | solution.py:231
  143.1 2.8 %collective-permute-start.16 = (bf16[640,512]{1,0:T(8,128)(2,1)}, bf16[640,512]{1,0:T(8,128)(2,1)}, u32[]{:S(2)}, u32[]{:S(2)}) collective-permute-start(bf16[640,512]{1,0:T(8,128)(2,1)} %collective-permute-done.15.rest_4_.rest_2_), channel_id=1, source_target_pairs={{0,1},{1,0},{2,3},{3,2},{4,5},{5,4},{6,7},{7,6},{8,9},{9,8},{10,11... | collective-permute-start | bytes 1966088 | tf_op jit(solution)/shard_map/ppermute | solution.py:231
  143.1 3.7 %collective-permute-start.18 = (bf16[640,512]{1,0:T(8,128)(2,1)}, bf16[640,512]{1,0:T(8,128)(2,1)}, u32[]{:S(2)}, u32[]{:S(2)}) collective-permute-start(bf16[640,512]{1,0:T(8,128)(2,1)} %collective-permute-done.17.rest_6_.rest_3_), channel_id=1, source_target_pairs={{0,1},{1,0},{2,3},{3,2},{4,5},{5,4},{6,7},{7,6},{8,9},{9,8},{10,11... | collective-permute-start | bytes 1966088 | tf_op jit(solution)/shard_map/ppermute | solution.py:231
  143.9 3.6 %collective-permute-start.11 = (bf16[512,512]{1,0:T(8,128)(2,1)}, bf16[512,512]{1,0:T(8,128)(2,1)S(1)}, u32[]{:S(2)}, u32[]{:S(2)}) collective-permute-start(bf16[512,512]{1,0:T(8,128)(2,1)} %bitcast.26), channel_id=1, source_target_pairs={{0,1},{1,0},{2,3},{3,2},{4,5},{5,4},{6,7},{7,6},{8,9},{9,8},{10,11... | collective-permute-start | bytes 1572872 | tf_op jit(solution)/shard_map/ppermute | solution.py:231
  197.6 20.6 %all-to-all-start.7 = ((bf16[8,64,512]{2,1,0:T(8,128)(2,1)}), bf16[8,64,512]{2,1,0:T(8,128)(2,1)S(1)}, u32[]{:S(2)}, u32[]{:S(2)}) async-start(bf16[8,64,512]{2,1,0:T(8,128)(2,1)} %bitcast.32), calls=%async_computation.7 | async-start | bytes 1048576 | tf_op jit(solution)/shard_map/all_to_all | solution.py:364
  (5 other events, 7.5 us)
